TPU v7x, 32 devices: a whole 2x2x4 slice. The times are simulated.
32 devices in a mesh: grp: 2 (over x), ep: 16 (over z, y, core).
Axes of the slice: x: 2, y: 2, z: 4, core: 2. Of those that a mesh axis runs over, the one named last changes fastest.
Arguments:
- sequence_input_rows: bfloat16 [224, 2048], P(('grp', 'ep')), parts along dimension 0, may hold values from -6 to 6
- value_key_state: float32 [224, 32, 64, 64], P(('grp', 'ep')), parts along dimension 0, may hold values from -4 to 4
- receptance_matrix: bfloat16 [2048, 2048], P(None, 'ep'), may hold values from -0.125 to 0.125
- key_matrix: bfloat16 [2048, 2048], P(None, 'ep'), may hold values from -0.125 to 0.125
- value_matrix: bfloat16 [2048, 2048], P(None, 'ep'), may hold values from -0.125 to 0.125
- decay_lowrank_input: bfloat16 [2048, 64], replicated, may hold values from -0.125 to 0.125
- decay_lowrank_output: bfloat16 [64, 2048], replicated, may hold values from -0.75 to 0.75
- decay_base_preact: float32 [2048], replicated, may hold values from -6 to -1
- context_rate_input: bfloat16 [2048, 64], replicated, may hold values from -0.125 to 0.125
- context_rate_output: bfloat16 [64, 2048], replicated, may hold values from -0.75 to 0.75
- context_rate_base: float32 [2048], replicated, may hold values from -4 to 4
- removal_key_scale: float32 [2048], replicated, may hold values from 0.1 to 1.9
- key_context_rate_blend: float32 [2048], replicated, may hold values from 0.1 to 1.9
- present_item_coefficient: float32 [32, 64], replicated, may hold values from -0.9 to 0.9
- head_norm_gain: float32 [2048], replicated, may hold values from 0.1 to 1.9
- mixer_output_matrix: bfloat16 [2048, 2048], P(None, 'ep'), may hold values from -0.125 to 0.125
- mixer_norm_gain: float32 [2048], replicated, may hold values from 0.1 to 1.9
- group_router_columns: bfloat16 [2048, 4], replicated, may hold values from -8 to 8
- expert_router_columns: bfloat16 [2048, 16], replicated, may hold values from -0.125 to 0.125
- expert_gate_matrix: bfloat16 [16, 2048, 256], P('ep'), may hold values from -0.125 to 0.125
- expert_up_matrix: bfloat16 [16, 2048, 256], P('ep'), may hold values from -0.125 to 0.125
- expert_down_matrix: bfloat16 [16, 256, 2048], P('ep'), may hold values from -0.375 to 0.375
- final_norm_gain: float32 [2048], replicated, may hold values from 0.1 to 1.9
- routes: int32 [224, 4], P(('grp', 'ep')), parts along dimension 0, may hold values from 0 to 15, as said below
Outputs:
- tokens_out: bfloat16 [224, 2048], P(('grp', 'ep')), parts along dimension 0
- next_recurrent_state: float32 [224, 32, 64, 64], P(('grp', 'ep')), parts along dimension 0
There are 2 independent parts, one for each index of `grp`. A program takes and returns all parts, laid end to end along the dimension named above; an argument that names none is the same for every part. Nothing has to cross between parts.
Inputs may be any that keep to these rules, and one draw needn't show every extreme that they name: `routes`: the 4 experts of a row are different and lie in the same group (expert // 4). In each aligned block of 7 rows (the rows of one device) no expert is named more than 2 times, and in every block some expert is named exactly 2 times.
All inputs are finite; a program needn't handle non-finite values.
Results may differ from a plain program's by a relative error of at most 0.0067.
Values may be sent and summed in bfloat16 or wider, within the bound.
A program may use at most 128 MiB of HBM per device.

v0:
```python
import jax
import jax.numpy as jnp
from jax import lax
from jax.sharding import PartitionSpec as P

CAP = 2


residual_scale = 8.0**0.25
norm_eps = 1e-05
group_eps = 0.00064


def layer_norm(values, norm_gain):
    center = jnp.mean(values, -1, keepdims=True)
    spread = jnp.mean(jnp.square(values - center), -1, keepdims=True)
    return (values - center) * lax.rsqrt(spread + norm_eps) * norm_gain


def token_mixer_step(
    sequence_input_rows,
    receptance_rows,
    key_projected_rows,
    value_projected_rows,
    value_key_state,
    decay_lowrank_input,
    decay_lowrank_output,
    decay_base_preact,
    context_rate_input,
    context_rate_output,
    context_rate_base,
    removal_key_scale,
    key_context_rate_blend,
    present_item_coefficient,
    head_norm_gain,
):
    series_entry_number = sequence_input_rows.shape[0]
    attention_subspace_number, subspace_dimension = present_item_coefficient.shape
    decay_low = jnp.tanh(
        jnp.dot(sequence_input_rows, decay_lowrank_input, preferred_element_type=jnp.float32)
    ).astype(jnp.bfloat16)
    decay_pre = decay_base_preact + jnp.dot(
        decay_low, decay_lowrank_output, preferred_element_type=jnp.float32
    )
    log_rate = -jax.nn.softplus(-decay_pre) - 0.5
    decay = jnp.exp(-jnp.exp(log_rate))
    iclr_low = jnp.dot(
        sequence_input_rows, context_rate_input, preferred_element_type=jnp.float32
    ).astype(jnp.bfloat16)
    iclr_rate = jax.nn.sigmoid(
        context_rate_base
        + jnp.dot(iclr_low, context_rate_output, preferred_element_type=jnp.float32)
    )

    def to_heads(values):
        return values.astype(jnp.float32).reshape(
            series_entry_number, attention_subspace_number, subspace_dimension
        )

    acceptance_subspaces = to_heads(receptance_rows)
    key_heads = to_heads(key_projected_rows)
    content_subspace_entries = to_heads(value_projected_rows)
    decay_heads = to_heads(decay)
    rate_heads = to_heads(iclr_rate)
    scaled_key = key_heads * removal_key_scale.reshape(
        attention_subspace_number, subspace_dimension
    )
    removal_dir = scaled_key * lax.rsqrt(
        jnp.sum(scaled_key * scaled_key, -1, keepdims=True) + 1e-06
    )
    adjusted_lookup_vector = key_heads * (
        1.0
        + (rate_heads - 1.0)
        * key_context_rate_blend.reshape(attention_subspace_number, subspace_dimension)
    )
    removed = jnp.einsum(
        "bhvk,bhk->bhv", value_key_state, removal_dir, precision=lax.Precision.HIGHEST
    )
    next_recurrent_state = (
        value_key_state * decay_heads[:, :, None, :]
        - removed[..., None] * (removal_dir * rate_heads)[:, :, None, :]
        + content_subspace_entries[..., None] * adjusted_lookup_vector[:, :, None, :]
    )
    readout = jnp.einsum(
        "bhvk,bhk->bhv", next_recurrent_state, acceptance_subspaces, precision=lax.Precision.HIGHEST
    )
    center = jnp.mean(readout, -1, keepdims=True)
    spread = jnp.mean(jnp.square(readout - center), -1, keepdims=True)
    standardized_entries = (
        (readout - center)
        * lax.rsqrt(spread + group_eps)
        * head_norm_gain.reshape(attention_subspace_number, subspace_dimension)
    )
    present_extra_reward = (
        jnp.sum(
            acceptance_subspaces * adjusted_lookup_vector * present_item_coefficient,
            -1,
            keepdims=True,
        )
        * content_subspace_entries
    )
    attention_mixing_outcome = (
        (standardized_entries + present_extra_reward)
        .reshape(series_entry_number, attention_subspace_number * subspace_dimension)
        .astype(jnp.bfloat16)
    )
    return (attention_mixing_outcome, next_recurrent_state)


def routing_gate(hidden, route_rows, chosen, group_router_columns, expert_router_columns):
    group_count = group_router_columns.shape[1]
    expert_count = expert_router_columns.shape[1]
    per_group = expert_count // group_count
    group_logits = jnp.dot(hidden, group_router_columns, preferred_element_type=jnp.float32)
    expert_logits = jnp.dot(hidden, expert_router_columns, preferred_element_type=jnp.float32)
    largest = jnp.max(group_logits, -1, keepdims=True)
    lifted = jnp.exp(group_logits - largest)
    in_group = (chosen // per_group)[:, None] == jnp.arange(group_count, dtype=jnp.int32)[None, :]
    group_prob = jnp.sum(jnp.where(in_group, lifted, 0.0), -1) / jnp.sum(lifted, -1)
    columns = jnp.arange(expert_count, dtype=jnp.int32)[None, :]
    chosen_logit = jnp.sum(jnp.where(chosen[:, None] == columns, expert_logits, 0.0), -1)
    total = jnp.zeros_like(chosen_logit)
    for slot in range(route_rows.shape[1]):
        other_logit = jnp.sum(
            jnp.where(route_rows[:, slot][:, None] == columns, expert_logits, 0.0), -1
        )
        total = total + jnp.exp(other_logit - chosen_logit)
    return group_prob / total


def expert_mlp(inputs, expert_weights):
    gate_weight, up_weight, down_weight = expert_weights
    gate_part = jnp.dot(inputs, gate_weight[0], preferred_element_type=jnp.float32)
    up_part = jnp.dot(inputs, up_weight[0], preferred_element_type=jnp.float32)
    act = (jax.nn.silu(gate_part) * up_part).astype(jnp.bfloat16)
    return jnp.dot(act, down_weight[0], preferred_element_type=jnp.float32).astype(jnp.bfloat16)


def by_exchange(hidden, routes, routers, expert_weights):
    series_entry_number, model_width = hidden.shape
    expert_count = routers[1].shape[1]
    is_named = routes[:, :, None] == jnp.arange(expert_count, dtype=jnp.int32)[None, None, :]
    per_row = jnp.sum(is_named.astype(jnp.int32), 1)
    before = jnp.cumsum(per_row, 0) - per_row
    slot_rank = jnp.sum(jnp.where(is_named, before[:, None, :], 0), -1)
    slot_index = routes * CAP + slot_rank
    placing = (
        slot_index[:, :, None] == jnp.arange(expert_count * CAP, dtype=jnp.int32)[None, None, :]
    ).astype(jnp.bfloat16)
    outgoing = jnp.einsum("rks,rd->sd", placing, hidden, preferred_element_type=jnp.float32)
    outgoing = outgoing.astype(jnp.bfloat16).reshape(expert_count, CAP, model_width)
    incoming = lax.all_to_all(outgoing, "ep", split_axis=0, concat_axis=0, tiled=True)
    flat_rows = incoming.reshape(-1, model_width)
    finished = expert_mlp(flat_rows, expert_weights).reshape(incoming.shape)
    returned = lax.all_to_all(finished, "ep", split_axis=0, concat_axis=0, tiled=True).reshape(
        expert_count * CAP, model_width
    )
    gate_values = jnp.stack(
        [
            routing_gate(hidden, routes, routes[:, slot], routers[0], routers[1])
            for slot in range(routes.shape[1])
        ],
        1,
    )
    picked = returned[slot_index]
    return jnp.sum(gate_values[:, :, None] * picked.astype(jnp.float32), 1)


def on_device(
    sequence_input_rows,
    value_key_state,
    receptance_matrix,
    key_matrix,
    value_matrix,
    decay_lowrank_input,
    decay_lowrank_output,
    decay_base_preact,
    context_rate_input,
    context_rate_output,
    context_rate_base,
    removal_key_scale,
    key_context_rate_blend,
    present_item_coefficient,
    head_norm_gain,
    mixer_output_matrix,
    mixer_norm_gain,
    group_router_columns,
    expert_router_columns,
    expert_gate_matrix,
    expert_up_matrix,
    expert_down_matrix,
    final_norm_gain,
    routes,
):
    section = lax.all_gather(sequence_input_rows, "ep", axis=0, tiled=True)
    columns = [
        jnp.dot(section, weight, preferred_element_type=jnp.float32).astype(jnp.bfloat16)
        for weight in (receptance_matrix, key_matrix, value_matrix)
    ]
    projected = jnp.stack(columns, axis=1)
    own_heads = lax.all_to_all(projected, "ep", split_axis=0, concat_axis=2, tiled=True)
    attention_mixing_outcome, next_recurrent_state = token_mixer_step(
        sequence_input_rows,
        own_heads[:, 0],
        own_heads[:, 1],
        own_heads[:, 2],
        value_key_state,
        decay_lowrank_input,
        decay_lowrank_output,
        decay_base_preact,
        context_rate_input,
        context_rate_output,
        context_rate_base,
        removal_key_scale,
        key_context_rate_blend,
        present_item_coefficient,
        head_norm_gain,
    )
    out_columns = jnp.dot(
        lax.all_gather(attention_mixing_outcome, "ep", axis=0, tiled=True),
        mixer_output_matrix,
        preferred_element_type=jnp.float32,
    ).astype(jnp.bfloat16)
    attn_out = lax.all_to_all(out_columns, "ep", split_axis=0, concat_axis=1, tiled=True)
    hidden = layer_norm(
        residual_scale * sequence_input_rows.astype(jnp.float32) + attn_out.astype(jnp.float32),
        mixer_norm_gain,
    ).astype(jnp.bfloat16)
    expert_weights = (expert_gate_matrix, expert_up_matrix, expert_down_matrix)
    routers = (group_router_columns, expert_router_columns)
    expert_sum = by_exchange(hidden, routes, routers, expert_weights)
    tokens_out = layer_norm(
        residual_scale * hidden.astype(jnp.float32) + expert_sum, final_norm_gain
    ).astype(jnp.bfloat16)
    return (tokens_out, next_recurrent_state)


def solution(mesh):
    in_specs = (
        P(("grp", "ep"), None),
        P(("grp", "ep"), None, None, None),
        P(None, "ep"),
        P(None, "ep"),
        P(None, "ep"),
        P(),
        P(),
        P(),
        P(),
        P(),
        P(),
        P(),
        P(),
        P(),
        P(),
        P(None, "ep"),
        P(),
        P(),
        P(),
        P("ep", None, None),
        P("ep", None, None),
        P("ep", None, None),
        P(),
        P(("grp", "ep"), None),
    )
    out_specs = (P(("grp", "ep"), None), P(("grp", "ep"), None, None, None))
    return jax.shard_map(
        on_device, mesh=mesh, in_specs=in_specs, out_specs=out_specs, check_vma=False
    )
```

profile of v0, /device:TPU:0, one launch (start us, length us, event | category | flops | bytes accessed | tf_op | source)
XLA Modules:
  0.0 138.3 jit_solution(8020242776843022416)
XLA Ops:
  0.6 25.0 %all-gather = bf16[16,7,2048]{2,1,0:T(8,128)(2,1)S(1)} all-gather(bf16[1,7,2048]{2,1,0:T(8,128)(2,1)} %bitcast.101), channel_id=1, replica_groups=mesh['grp'=2,'ep'=16] {'ep'}, dimensions={0}, use_global_device_ids=true | all-gather | bytes 487424 | tf_op jit(solution)/shard_map/all_gather | solution.py:195
  25.6 0.2 reshape.474
  25.8 1.3 fusion.10
  27.1 1.3 fusion.11
  28.4 1.3 fusion.9
  29.7 0.7 copy.40
  30.4 3.5 %all-to-all-start = ((bf16[112,3,128]{2,1,0:T(4,128)(2,1)}), bf16[112,3,128]{2,1,0:T(4,128)(2,1)S(1)}, u32[]{:S(2)}, u32[]{:S(2)}) async-start(bf16[112,3,128]{2,1,0:T(4,128)(2,1)} %copy.40), calls=%async_computation | async-start | bytes 229376 | tf_op jit(solution)/shard_map/all_to_all | solution.py:201
  34.0 0.8 copy.43
  34.9 0.3 select_reduce_fusion
  35.1 1.4 %fusion.4 = f32[7,2048]{1,0:T(8,128)S(1)} fusion(bf16[64,2048]{1,0:T(8,128)(2,1)} %param.33, bf16[7,2048]{1,0:T(8,128)(2,1)} %param.24, bf16[2048,64]{0,1:T(8,128)(2,1)} %param.32, f32[2048]{0:T(1024)} %param.34), kind=kOutput, calls=%fused_computation.9 | convolution fusion | flops 3727808 | bytes 618496 | tf_op jit(solution)/shard_map/dot_general | solution.py:52
  36.6 1.5 %fusion.24 = f32[7,2048]{1,0:T(8,128)S(1)} fusion(bf16[64,2048]{1,0:T(8,128)(2,1)} %param.30, bf16[7,2048]{1,0:T(8,128)(2,1)} %param.24, bf16[2048,64]{0,1:T(8,128)(2,1)} %param.29, f32[2048]{0:T(1024)} %param.31), kind=kOutput, calls=%fused_computation.45 | convolution fusion | flops 3828160 | bytes 618496 | tf_op jit(solution)/shard_map/dot_general | solution.py:42
  38.1 0.8 slice_bitcast_fusion.2
  38.9 0.8 mul.214
  39.8 0.8 mul.225
  40.6 0.8 mul.233
  41.9 0.1 multiply_reduce_fusion.2
  42.2 13.6 %fusion.48 = f32[7,32,1,64]{3,2,1,0:T(1,128)S(1)} fusion(f32[7,32,64,1]{2,3,1,0:T(1,128)S(1)} %bitcast.104, f32[7,32,64,64]{3,2,1,0:T(8,128)} %param.25), kind=kOutput, calls=%fused_computation.134 | convolution fusion | flops 11010048 | bytes 3784704 | tf_op jit(solution)/shard_map/bhvk,bhk->bhv/dot_general | solution.py:76
  55.9 7.9 %multiply_add_fusion = f32[7,32,64,64]{3,2,1,0:T(8,128)S(1)} fusion(f32[7,32,64,64]{3,2,1,0:T(8,128)} %param.25, f32[7,32,64]{2,1,0:T(8,128)S(1)} %get-tuple-element.15, f32[7,32,64]{2,1,0:T(8,128)S(1)} %reshape.448, f32[7,32,64]{2,1,0:T(8,128)S(1)} %get-tuple-element.13, f32[7,32,64]{2,1,0:T(8,128)S(1)} %bitcast.103, f32[7,32,64]{2,1,0:T(8,128)S(1)} %mul.211), kind=kLoop, calls=%fused_computation.2 | loop fusion | flops 4587520 | bytes 7626752 | tf_op jit(solution)/shard_map/add | solution.py:80
  63.8 3.0 %copy-done.1 = f32[7,32,64,64]{3,2,1,0:T(8,128)} copy-done((f32[7,32,64,64]{3,2,1,0:T(8,128)}, f32[7,32,64,64]{3,2,1,0:T(8,128)S(1)}, u32[]{:S(2)}) %copy-start.1) | copy-done | bytes 3670040
  66.9 5.8 %fusion.49 = f32[7,32,1,64]{3,2,1,0:T(1,128)S(1)} fusion(f32[7,32,64,64]{3,2,1,0:T(8,128)S(1)} %multiply_add_fusion, bf16[7,32,64,1]{2,3,1,0:T(2,128)(2,1)S(1)} %reshape.483), kind=kOutput, calls=%fused_computation.135 | convolution fusion | flops 11010048 | bytes 3756032 | tf_op jit(solution)/shard_map/bhvk,bhk->bhv/dot_general | solution.py:84
  72.7 0.1 reduce_sum.203
  72.8 0.2 multiply_reduce_fusion.1
  73.0 0.5 fusion.8
  73.5 0.1 reshape.475
  73.6 23.2 %all-gather.1 = bf16[16,7,2048]{2,1,0:T(8,128)(2,1)S(1)} all-gather(bf16[1,7,2048]{2,1,0:T(8,128)(2,1)S(1)} %reshape.475), channel_id=1, replica_groups=mesh['grp'=2,'ep'=16] {'ep'}, dimensions={0}, use_global_device_ids=true | all-gather | bytes 487424 | tf_op jit(solution)/shard_map/all_gather | solution.py:220
  96.8 0.2 reshape.476
  97.0 1.3 convolution_convert_fusion.2
  98.3 0.6 all_to_all.33
  98.9 3.5 %all-to-all-start.1 = ((bf16[16,7,128]{2,1,0:T(8,128)(2,1)}), bf16[16,7,128]{2,1,0:T(8,128)(2,1)S(1)}, u32[]{:S(2)}, u32[]{:S(2)}) async-start(bf16[16,7,128]{2,1,0:T(8,128)(2,1)} %all_to_all.33), calls=%async_computation.1 | async-start | bytes 65536 | tf_op jit(solution)/shard_map/all_to_all | solution.py:224
  102.4 6.6 %all-to-all-done.1 = bf16[16,7,128]{2,1,0:T(8,128)(2,1)S(1)} async-done(((bf16[16,7,128]{2,1,0:T(8,128)(2,1)}), bf16[16,7,128]{2,1,0:T(8,128)(2,1)S(1)}, u32[]{:S(2)}, u32[]{:S(2)}) %all-to-all-start.1) | async-done | bytes 28704 | tf_op jit(solution)/shard_map/all_to_all | solution.py:224
  109.0 0.1 fusion.26
  109.2 0.2 multiply_reduce_fusion.4
  109.5 0.2 fusion.50
  109.7 0.7 reshape.443
  110.4 3.5 %all-to-all-start.2 = ((bf16[16,2,2048]{2,1,0:T(2,128)(2,1)}), bf16[16,2,2048]{2,1,0:T(2,128)(2,1)S(1)}, u32[]{:S(2)}, u32[]{:S(2)}) async-start(bf16[16,2,2048]{2,1,0:T(2,128)(2,1)} %reshape.443), calls=%async_computation.2 | async-start | bytes 262144 | tf_op jit(solution)/shard_map/all_to_all | solution.py:152
  114.0 0.1 fusion.47
  114.2 0.3 select_reduce_fusion.4
  114.4 7.4 %all-to-all-done.2 = bf16[16,2,2048]{2,1,0:T(2,128)(2,1)S(1)} async-done(((bf16[16,2,2048]{2,1,0:T(2,128)(2,1)}), bf16[16,2,2048]{2,1,0:T(2,128)(2,1)S(1)}, u32[]{:S(2)}, u32[]{:S(2)}) %all-to-all-start.2) | async-done | bytes 131104 | tf_op jit(solution)/shard_map/all_to_all | solution.py:152
  121.9 1.5 %fusion.17 = f32[32,256]{1,0:T(8,128)S(1)} fusion(bf16[32,2048]{1,0:T(8,128)(2,1)S(1)} %reshape.444, bf16[1,2048,256]{2,1,0:T(8,128)(2,1)} %param.43), kind=kOutput, calls=%fused_computation.29 | convolution fusion | flops 33554432 | bytes 1212416 | tf_op jit(solution)/shard_map/dot_general | solution.py:133
  123.4 0.7 convolution_convert_fusion
  124.1 0.8 reshape.445
  124.9 3.5 %all-to-all-start.3 = ((bf16[16,2,2048]{2,1,0:T(2,128)(2,1)}), bf16[16,2,2048]{2,1,0:T(2,128)(2,1)S(1)}, u32[]{:S(2)}, u32[]{:S(2)}) async-start(bf16[16,2,2048]{2,1,0:T(2,128)(2,1)} %reshape.445), calls=%async_computation.3 | async-start | bytes 262144 | tf_op jit(solution)/shard_map/all_to_all | solution.py:155
  128.6 7.7 %all-to-all-done.3 = bf16[16,2,2048]{2,1,0:T(2,128)(2,1)S(1)} async-done(((bf16[16,2,2048]{2,1,0:T(2,128)(2,1)}), bf16[16,2,2048]{2,1,0:T(2,128)(2,1)S(1)}, u32[]{:S(2)}, u32[]{:S(2)}) %all-to-all-start.3) | async-done | bytes 131104 | tf_op jit(solution)/shard_map/all_to_all | solution.py:155
  136.3 0.6 gather_fusion
  137.1 0.2 multiply_reduce_fusion
  137.3 0.1 fusion.32
  137.4 0.2 multiply_reduce_fusion.3
  137.6 0.7 multiply_convert_fusion
  (50 shorter events, 1.5 us)
Async XLA Ops:
  0.6 122.8 %copy-start = (bf16[1,256,2048]{2,1,0:T(8,128)(2,1)S(1)}, bf16[1,256,2048]{2,1,0:T(8,128)(2,1)}, u32[]{:S(2)}) copy-start(bf16[1,256,2048]{2,1,0:T(8,128)(2,1)} %param.45) | copy-start | bytes 3145732
  30.4 11.1 %all-to-all-start = ((bf16[112,3,128]{2,1,0:T(4,128)(2,1)}), bf16[112,3,128]{2,1,0:T(4,128)(2,1)S(1)}, u32[]{:S(2)}, u32[]{:S(2)}) async-start(bf16[112,3,128]{2,1,0:T(4,128)(2,1)} %copy.40), calls=%async_computation | async-start | bytes 229376 | tf_op jit(solution)/shard_map/all_to_all | solution.py:201
  63.8 3.1 %copy-start.1 = (f32[7,32,64,64]{3,2,1,0:T(8,128)}, f32[7,32,64,64]{3,2,1,0:T(8,128)S(1)}, u32[]{:S(2)}) copy-start(f32[7,32,64,64]{3,2,1,0:T(8,128)S(1)} %multiply_add_fusion) | copy-start | bytes 11010052
  66.8 6.2 %copy-start.4 = (f32[32,64]{1,0:T(8,128)S(1)}, f32[32,64]{1,0:T(8,128)}, u32[]{:S(2)}) copy-start(f32[32,64]{1,0:T(8,128)} %param.37) | copy-start | bytes 24580
  66.8 42.2 %copy-start.2 = (bf16[7,2048]{1,0:T(8,128)(2,1)S(1)}, bf16[7,2048]{1,0:T(8,128)(2,1)}, u32[]{:S(2)}) copy-start(bf16[7,2048]{1,0:T(8,128)(2,1)} %param.24) | copy-start | bytes 86020
  66.8 42.5 %copy-start.6 = (f32[2048]{0:T(1024)S(1)}, f32[2048]{0:T(1024)}, u32[]{:S(2)}) copy-start(f32[2048]{0:T(1024)} %param.40) | copy-start | bytes 24580
  66.8 47.1 %copy-start.8 = (bf16[2048,4]{0,1:T(4,128)(2,1)S(1)}, bf16[2048,4]{0,1:T(4,128)(2,1)}, u32[]{:S(2)}) copy-start(bf16[2048,4]{0,1:T(4,128)(2,1)} %param.41) | copy-start | bytes 49156
  66.8 47.3 %copy-start.7 = (bf16[2048,16]{0,1:T(8,128)(2,1)S(1)}, bf16[2048,16]{0,1:T(8,128)(2,1)}, u32[]{:S(2)}) copy-start(bf16[2048,16]{0,1:T(8,128)(2,1)} %param.42) | copy-start | bytes 196612
  66.9 56.5 %copy-start.3 = (bf16[1,2048,256]{2,1,0:T(8,128)(2,1)S(1)}, bf16[1,2048,256]{2,1,0:T(8,128)(2,1)}, u32[]{:S(2)}) copy-start(bf16[1,2048,256]{2,1,0:T(8,128)(2,1)} %param.44) | copy-start | bytes 3145732
  72.7 65.0 %copy-start.5 = (f32[2048]{0:T(1024)S(1)}, f32[2048]{0:T(1024)}, u32[]{:S(2)}) copy-start(f32[2048]{0:T(1024)} %param.46) | copy-start | bytes 24580
  98.9 10.1 %all-to-all-start.1 = ((bf16[16,7,128]{2,1,0:T(8,128)(2,1)}), bf16[16,7,128]{2,1,0:T(8,128)(2,1)S(1)}, u32[]{:S(2)}, u32[]{:S(2)}) async-start(bf16[16,7,128]{2,1,0:T(8,128)(2,1)} %all_to_all.33), calls=%async_computation.1 | async-start | bytes 65536 | tf_op jit(solution)/shard_map/all_to_all | solution.py:224
  110.4 11.4 %all-to-all-start.2 = ((bf16[16,2,2048]{2,1,0:T(2,128)(2,1)}), bf16[16,2,2048]{2,1,0:T(2,128)(2,1)S(1)}, u32[]{:S(2)}, u32[]{:S(2)}) async-start(bf16[16,2,2048]{2,1,0:T(2,128)(2,1)} %reshape.443), calls=%async_computation.2 | async-start | bytes 262144 | tf_op jit(solution)/shard_map/all_to_all | solution.py:152
  124.9 11.4 %all-to-all-start.3 = ((bf16[16,2,2048]{2,1,0:T(2,128)(2,1)}), bf16[16,2,2048]{2,1,0:T(2,128)(2,1)S(1)}, u32[]{:S(2)}, u32[]{:S(2)}) async-start(bf16[16,2,2048]{2,1,0:T(2,128)(2,1)} %reshape.445), calls=%async_computation.3 | async-start | bytes 262144 | tf_op jit(solution)/shard_map/all_to_all | solution.py:155
where the time goes:
time: 139 us; the launch traced here: 138 us
  blocking collectives  48.2 us (35%)
  matrix products  30.5 us (22%)
  waiting for transfers between devices  21.7 us (16%)
  starting transfers between devices  14 us (10%)
  other arithmetic  12 us (9%)
  local copies, waits for them, and re-layouts  11 us (8%)
    all_gather x1, blocking collectives, on_device(): section = lax.all_gather(sequence_input_rows, 'ep', axis=0, tiled=True)  25 us
    all_gather x1, blocking collectives, on_device(): lax.all_gather(attention_mixing_outcome, 'ep', axis=0, tiled=True)  23.2 us
    dot_general x1, matrix products, token_mixer_step(): jnp.einsum('bhvk,bhk->bhv', value_key_state, removal_dir, precision=lax.P...  13.6 us
    add x1, other arithmetic, token_mixer_step(): value_key_state * decay_heads[:, :, None, :]  7.89 us
    all_to_all x1, waiting for transfers between devices, by_exchange(): lax.all_to_all(finished, 'ep', split_axis=0, concat_axis=0, tiled=True)  7.72 us
    all_to_all x1, waiting for transfers between devices, by_exchange(): lax.all_to_all(outgoing, 'ep', split_axis=0, concat_axis=0, tiled=True)  7.39 us
    all_to_all x1, waiting for transfers between devices, on_device(): lax.all_to_all(out_columns, 'ep', split_axis=0, concat_axis=1, tiled=True)  6.58 us
    dot_general x1, matrix products, token_mixer_step(): jnp.einsum('bhvk,bhk->bhv', next_recurrent_state, acceptance_subspaces, p...  5.79 us
  transfers between devices with their start and end apart: 4, of which 3 were waited for; matrix products, arithmetic and copies ran while one was open for 6% of the time, Pallas kernels for 0%

commit v1 on v0

v1 whole, which is shorter than its diff:
```python
import functools

import jax
import jax.numpy as jnp
from jax import lax
from jax.experimental import pallas as pl
from jax.experimental.pallas import tpu as pltpu
from jax.sharding import PartitionSpec as P

CAP = 2
PAD = 8
LANES = 128

residual_scale = 8.0**0.25
norm_eps = 1e-05
group_eps = 0.00064

MESH = pl.DeviceIdType.MESH
F32 = jnp.float32
BF16 = jnp.bfloat16
HIGHEST = lax.Precision.HIGHEST


def layer_norm(values, norm_gain):
    center = jnp.mean(values, -1, keepdims=True)
    spread = jnp.mean(jnp.square(values - center), -1, keepdims=True)
    return (values - center) * lax.rsqrt(spread + norm_eps) * norm_gain


def contract(a, b, dims, precision=None):
    return lax.dot_general(a, b, ((dims[:1], dims[1:]), ((), ())), precision=precision,
                           preferred_element_type=F32)


def sigmoid(values):
    return 1.0 / (1.0 + jnp.exp(-values))


def each_peer(n, me, act):
    def body(d, carry):
        act(lax.rem(me + d, n))
        return carry

    lax.fori_loop(1, n, body, 0)


def enter(n, me):
    barrier = pltpu.get_barrier_semaphore()
    each_peer(n, me, lambda peer: pl.semaphore_signal(
        barrier, inc=1, device_id={"ep": peer}, device_id_type=MESH))
    pl.semaphore_wait(barrier, n - 1)


class Exchange:
    def __init__(self, n, me, source_of, landing, send, recv):
        self.n, self.me, self.source_of = n, me, source_of
        self.landing, self.send, self.recv = landing, send, recv

    def start(self, peer):
        pltpu.make_async_remote_copy(
            src_ref=self.source_of(peer),
            dst_ref=self.landing.at[self.me],
            send_sem=self.send.at[peer],
            recv_sem=self.recv.at[self.me],
            device_id={"ep": peer},
            device_id_type=MESH,
        ).start()

    def start_all(self):
        each_peer(self.n, self.me, self.start)

    def incoming(self, peer):
        return pltpu.make_async_remote_copy(
            src_ref=self.source_of(peer),
            dst_ref=self.landing.at[peer],
            send_sem=self.send.at[peer],
            recv_sem=self.recv.at[peer],
            device_id={"ep": peer},
            device_id_type=MESH,
        )

    def wait_recv(self, then=None):
        def body(d, carry):
            peer = lax.rem(self.me + self.n - d, self.n)
            self.incoming(peer).wait_recv()
            if then is not None:
                then(peer)
            return carry

        lax.fori_loop(1, self.n, body, 0)

    def wait_send(self):
        each_peer(self.n, self.me, lambda peer: self.incoming(peer).wait_send())


def project_kernel(
    n, x_ref, wr, wk, wv, dli, dlo, dbase, cri, cro, cbase,
    rkv_out, decay_out, rate_out,
    weights, dli_v, dlo_v, cri_v, cro_v, gathered, rows, outs, back,
    local, send1, recv1, send2, recv2,
):
    me = lax.axis_index("ep")
    series, _ = x_ref.shape
    width = wr.shape[1]
    loads = [
        pltpu.make_async_copy(src, dst, local.at[i])
        for i, (src, dst) in enumerate([
            (dli, dli_v), (cri, cri_v), (dlo, dlo_v), (cro, cro_v),
            (wr, weights.at[0]), (wk, weights.at[1]), (wv, weights.at[2]),
        ])
    ]
    for load in loads:
        load.start()
    enter(n, me)
    gather = Exchange(n, me, lambda peer: x_ref, gathered, send1, recv1)
    gather.start_all()

    rows[...] = jnp.zeros_like(rows)

    def place(source, block):
        rows[pl.ds(pl.multiple_of(source * PAD, PAD), series), :] = block.astype(F32)

    place(me, x_ref[...])
    own = rows[pl.ds(pl.multiple_of(me * PAD, PAD), PAD), :].astype(BF16)
    for load in loads[:4]:
        load.wait()
    decay_low = jnp.tanh(contract(own, dli_v[...], (1, 1))).astype(BF16)
    decay_pre = dbase[...] + contract(decay_low, dlo_v[...], (1, 0))
    decay_out[...] = jnp.exp(sigmoid(decay_pre) * -(2.718281828459045**-0.5))
    iclr_low = contract(own, cri_v[...], (1, 1)).astype(BF16)
    rate_out[...] = sigmoid(cbase[...] + contract(iclr_low, cro_v[...], (1, 0)))
    for load in loads[4:]:
        load.wait()

    gather.wait_recv(lambda peer: place(peer, gathered[peer]))
    lhs = rows[...].astype(BF16)
    for c in range(3):
        columns = jnp.dot(lhs, weights[c], preferred_element_type=F32)
        outs[:, c] = columns.reshape(n, PAD, width).astype(BF16)
    spread = Exchange(n, me, lambda peer: outs.at[peer], back, send2, recv2)
    spread.start_all()
    back[me] = outs[me]
    spread.wait_recv()
    for source in range(n):
        for c in range(3):
            rkv_out[c, :, source * width : (source + 1) * width] = back[source, c].astype(F32)
    gather.wait_send()
    spread.wait_send()


def mixer_kernel(
    state, rkv, decay_ref, rate_ref, scale_ref, blend_ref, coef_ref, gain_ref,
    mixed_out, next_out,
):
    step = pl.program_id(0)
    series, per_step, head, _ = state.shape
    value_columns = jnp.transpose(rkv[2])
    lane = lax.broadcasted_iota(jnp.int32, (head, LANES), 1)
    pieces = []
    for h in range(per_step):
        part = slice(h * head, (h + 1) * head)
        r, k, v = (rkv[c][:, part] for c in range(3))
        decay, rate = decay_ref[:, part], rate_ref[:, part]
        scaled = k * scale_ref[:, part]
        removal = scaled * lax.rsqrt(jnp.sum(scaled * scaled, -1, keepdims=True) + 1e-06)
        key_mod = k * (1.0 + (rate - 1.0) * blend_ref[:, part])
        written = removal * rate
        readouts = jnp.zeros((head, LANES), F32)
        for t in range(series):
            row = slice(t, t + 1)
            block = state[t, h]
            removed = jnp.sum(block * removal[row], -1, keepdims=True)
            after = (
                block * decay[row]
                - removed * written[row]
                + value_columns[part, row] * key_mod[row]
            )
            next_out[t, h] = after
            readout = jnp.sum(after * r[row], -1, keepdims=True)
            readouts = jnp.where(lane == t, readout, readouts)
        readout = jnp.transpose(readouts)[:PAD]
        center = jnp.mean(readout, -1, keepdims=True)
        spread = jnp.mean(jnp.square(readout - center), -1, keepdims=True)
        standard = (readout - center) * lax.rsqrt(spread + group_eps) * gain_ref[:, part]
        coef = coef_ref[pl.ds(step * per_step + h, 1), :]
        present = jnp.sum(r * key_mod * coef, -1, keepdims=True) * v
        pieces.append(standard + present)
    mixed_out[...] = jnp.concatenate(pieces, axis=1).astype(BF16)


def finish_kernel(
    n, mixed, x_ref, routes, norm_gain, group_router, expert_router, final_gain,
    w_out, w_gate, w_up, w_down,
    tokens_out,
    wo_v, wg_v, wu_v, wd_v, gathered, outs, back, attn, resid, flat, away, arrived, home,
    landed, local, send1, recv1, send2, recv2, send3, recv3, send4, recv4,
):
    me = lax.axis_index("ep")
    series, model = x_ref.shape
    width = w_out.shape[1]
    experts = expert_router.shape[0]
    groups = group_router.shape[0]
    top = routes.shape[0]
    loads = [
        pltpu.make_async_copy(src, dst, local.at[i])
        for i, (src, dst) in enumerate(
            [(w_out, wo_v), (w_gate, wg_v), (w_up, wu_v), (w_down, wd_v)]
        )
    ]
    for load in loads:
        load.start()
    enter(n, me)
    gather = Exchange(n, me, lambda peer: mixed, gathered, send1, recv1)
    gather.start_all()
    gathered[me] = mixed[...]
    resid[...] = jnp.zeros_like(resid)
    resid[:series, :] = x_ref[...].astype(F32)

    slots = experts * CAP
    slot_ids = lax.broadcasted_iota(jnp.int32, (slots, PAD), 0)
    named = jnp.zeros((slots, PAD), F32)
    rank = jnp.zeros((slots, PAD), F32)
    for k in range(top):
        offset = slot_ids - routes[k : k + 1, :] * CAP
        match = (offset >= 0) & (offset < CAP)
        named = named + jnp.where(match, 1.0, 0.0)
        rank = rank + jnp.where(match, offset.astype(F32), 0.0)
    earlier = (
        lax.broadcasted_iota(jnp.int32, (PAD, PAD), 0)
        < lax.broadcasted_iota(jnp.int32, (PAD, PAD), 1)
    ).astype(F32)
    before = contract(named, earlier, (1, 0))
    placing = jnp.where(jnp.abs(before - rank) < 0.5, named, 0.0)
    ahead = lax.broadcasted_iota(jnp.int32, (slots, experts), 0) - CAP * (
        lax.broadcasted_iota(jnp.int32, (slots, experts), 1)
    )
    repeat = jnp.where((ahead >= 0) & (ahead < CAP), 1.0, 0.0)

    loads[0].wait()
    gather.wait_recv()
    lhs = gathered[...].astype(F32).reshape(n * PAD, model).astype(BF16)
    columns = jnp.dot(lhs, wo_v[...], preferred_element_type=F32)
    outs[...] = columns.reshape(n, PAD, width).astype(BF16)
    spread = Exchange(n, me, lambda peer: outs.at[peer], back, send2, recv2)
    spread.start_all()
    back[me] = outs[me]
    spread.wait_recv()
    for source in range(n):
        attn[:, source * width : (source + 1) * width] = back[source].astype(F32)
    hidden = layer_norm(residual_scale * resid[...] + attn[...], norm_gain[...]).astype(BF16)

    flat[...] = contract(placing.astype(BF16), hidden, (1, 0))

    for e in range(n):
        away[e] = flat[e * CAP : (e + 1) * CAP, :].astype(BF16)
    dispatch = Exchange(n, me, lambda peer: away.at[peer], arrived, send3, recv3)
    dispatch.start_all()
    arrived[me] = away[me]

    group_logits = contract(group_router[...], hidden, (1, 1))
    expert_logits = contract(
        repeat, contract(expert_router[...], hidden, (1, 1)), (1, 0), HIGHEST
    )
    lifted = jnp.exp(group_logits - jnp.max(group_logits, 0, keepdims=True))
    group_ids = lax.broadcasted_iota(jnp.int32, (groups, PAD), 0) * (experts // groups)
    first = routes[0:1, :]
    in_group = (first >= group_ids) & (first < group_ids + experts // groups)
    group_prob = jnp.sum(jnp.where(in_group, lifted, 0.0), 0, keepdims=True) / jnp.sum(
        lifted, 0, keepdims=True
    )
    is_named = named > 0.5
    highest = jnp.max(jnp.where(is_named, expert_logits, -1e30), 0, keepdims=True)
    raised = jnp.where(is_named, jnp.exp(expert_logits - highest), 0.0)
    total = jnp.sum(raised, 0, keepdims=True) / CAP
    gates = group_prob * raised / jnp.where(total > 0.0, total, 1.0)
    weights = gates * placing

    for load in loads[1:]:
        load.wait()

    dispatch.wait_recv()
    for s in range(n):
        flat[s * CAP : (s + 1) * CAP, :] = arrived[s].astype(F32)
    rows = flat[...].astype(BF16)
    gate_part = jnp.dot(rows, wg_v[0], preferred_element_type=F32)
    up_part = jnp.dot(rows, wu_v[0], preferred_element_type=F32)
    act = (gate_part * sigmoid(gate_part) * up_part).astype(BF16)
    flat[...] = jnp.dot(act, wd_v[0], preferred_element_type=F32)

    for s in range(n):
        home[s] = flat[s * CAP : (s + 1) * CAP, :].astype(BF16)
    giveback = Exchange(n, me, lambda peer: home.at[peer], landed, send4, recv4)
    giveback.start_all()
    landed[me] = home[me]

    giveback.wait_recv()
    for e in range(n):
        flat[e * CAP : (e + 1) * CAP, :] = landed[e].astype(F32)
    expert_sum = contract(weights, flat[...], (0, 0), HIGHEST)
    tokens = layer_norm(residual_scale * hidden.astype(F32) + expert_sum, final_gain[...])
    tokens_out[...] = tokens[:series].astype(BF16)
    gather.wait_send()
    spread.wait_send()
    dispatch.wait_send()
    giveback.wait_send()


VMEM = pl.BlockSpec(memory_space=pltpu.VMEM)
ANY = pl.BlockSpec(memory_space=pl.ANY)
MIB = 1024 * 1024


def on_device(
    n,
    sequence_input_rows,
    value_key_state,
    receptance_matrix,
    key_matrix,
    value_matrix,
    decay_lowrank_input,
    decay_lowrank_output,
    decay_base_preact,
    context_rate_input,
    context_rate_output,
    context_rate_base,
    removal_key_scale,
    key_context_rate_blend,
    present_item_coefficient,
    head_norm_gain,
    mixer_output_matrix,
    mixer_norm_gain,
    group_router_columns,
    expert_router_columns,
    expert_gate_matrix,
    expert_up_matrix,
    expert_down_matrix,
    final_norm_gain,
    routes,
):
    series, model = sequence_input_rows.shape
    heads, head = present_item_coefficient.shape
    inner = heads * head
    width = receptance_matrix.shape[1]
    out_width = mixer_output_matrix.shape[1]
    experts = expert_router_columns.shape[1]
    low_d, low_a = decay_lowrank_input.shape[1], context_rate_input.shape[1]
    hidden_units = expert_gate_matrix.shape[2]
    assert experts == n

    def row(values):
        return values.reshape(1, -1)

    dma = pltpu.SemaphoreType.DMA
    rkv, decay, rate = pl.pallas_call(
        functools.partial(project_kernel, n),
        out_shape=[
            jax.ShapeDtypeStruct((3, PAD, inner), F32),
            jax.ShapeDtypeStruct((PAD, inner), F32),
            jax.ShapeDtypeStruct((PAD, inner), F32),
        ],
        in_specs=[VMEM, ANY, ANY, ANY, ANY, ANY, VMEM, ANY, ANY, VMEM],
        out_specs=[VMEM] * 3,
        scratch_shapes=[
            pltpu.VMEM((3, model, width), BF16),
            pltpu.VMEM((low_d, model), BF16),
            pltpu.VMEM((low_d, inner), BF16),
            pltpu.VMEM((low_a, model), BF16),
            pltpu.VMEM((low_a, inner), BF16),
            pltpu.VMEM((n, series, model), BF16),
            pltpu.VMEM((n * PAD, model), F32),
            pltpu.VMEM((n, 3, PAD, width), BF16),
            pltpu.VMEM((n, 3, PAD, width), BF16),
            dma((7,)),
        ]
        + [dma((n,))] * 4,
        compiler_params=pltpu.CompilerParams(
            collective_id=0, has_side_effects=True, vmem_limit_bytes=32 * MIB
        ),
        name="project",
    )(
        sequence_input_rows,
        receptance_matrix,
        key_matrix,
        value_matrix,
        decay_lowrank_input.T,
        decay_lowrank_output,
        row(decay_base_preact),
        context_rate_input.T,
        context_rate_output,
        row(context_rate_base),
    )

    per_step = LANES // head

    def lanes(rows):
        return pl.BlockSpec((rows, LANES), lambda s: (0, s))

    state_spec = pl.BlockSpec((series, per_step, head, head), lambda s: (0, s, 0, 0))
    mixed, next_recurrent_state = pl.pallas_call(
        mixer_kernel,
        grid=(heads // per_step,),
        out_shape=[
            jax.ShapeDtypeStruct((PAD, inner), BF16),
            jax.ShapeDtypeStruct(value_key_state.shape, F32),
        ],
        in_specs=[
            state_spec,
            pl.BlockSpec((3, PAD, LANES), lambda s: (0, 0, s)),
            lanes(PAD),
            lanes(PAD),
            lanes(1),
            lanes(1),
            pl.BlockSpec((heads, head), lambda s: (0, 0)),
            lanes(1),
        ],
        out_specs=[lanes(PAD), state_spec],
        name="mixer",
    )(
        value_key_state,
        rkv,
        decay,
        rate,
        row(removal_key_scale),
        row(key_context_rate_blend),
        present_item_coefficient,
        row(head_norm_gain),
    )

    routes_t = jnp.pad(routes.T, ((0, 0), (0, PAD - series)), constant_values=-1)
    tokens_out = pl.pallas_call(
        functools.partial(finish_kernel, n),
        out_shape=jax.ShapeDtypeStruct((series, model), BF16),
        in_specs=[VMEM] * 7 + [ANY] * 4,
        out_specs=VMEM,
        scratch_shapes=[
            pltpu.VMEM((inner, out_width), BF16),
            pltpu.VMEM((1, model, hidden_units), BF16),
            pltpu.VMEM((1, model, hidden_units), BF16),
            pltpu.VMEM((1, hidden_units, model), BF16),
            pltpu.VMEM((n, PAD, inner), BF16),
            pltpu.VMEM((n, PAD, out_width), BF16),
            pltpu.VMEM((n, PAD, out_width), BF16),
            pltpu.VMEM((PAD, model), F32),
            pltpu.VMEM((PAD, model), F32),
            pltpu.VMEM((experts * CAP, model), F32),
        ]
        + [pltpu.VMEM((n, CAP, model), BF16)] * 4
        + [dma((4,))]
        + [dma((n,))] * 8,
        compiler_params=pltpu.CompilerParams(
            collective_id=1, has_side_effects=True, vmem_limit_bytes=32 * MIB
        ),
        name="finish",
    )(
        mixed,
        sequence_input_rows,
        routes_t,
        row(mixer_norm_gain),
        group_router_columns.T,
        expert_router_columns.T,
        row(final_norm_gain),
        mixer_output_matrix,
        expert_gate_matrix,
        expert_up_matrix,
        expert_down_matrix,
    )
    return (tokens_out, next_recurrent_state)


def solution(mesh):
    in_specs = (
        P(("grp", "ep"), None),
        P(("grp", "ep"), None, None, None),
        P(None, "ep"),
        P(None, "ep"),
        P(None, "ep"),
        P(),
        P(),
        P(),
        P(),
        P(),
        P(),
        P(),
        P(),
        P(),
        P(),
        P(None, "ep"),
        P(),
        P(),
        P(),
        P("ep", None, None),
        P("ep", None, None),
        P("ep", None, None),
        P(),
        P(("grp", "ep"), None),
    )
    out_specs = (P(("grp", "ep"), None), P(("grp", "ep"), None, None, None))
    return jax.shard_map(
        functools.partial(on_device, mesh.shape["ep"]),
        mesh=mesh, in_specs=in_specs, out_specs=out_specs, check_vma=False,
    )
```

time: 139 us -> 125 us (0.90)
  Pallas kernels: 0 us -> 110 us
  blocking collectives: 48.2 us -> 0 us
  matrix products: 30.5 us -> 0 us
  waiting for transfers between devices: 21.7 us -> 0 us
  starting transfers between devices: 14 us -> 0 us
  other arithmetic: 12 us -> 0 us
  local copies, waits for them, and re-layouts: 11 us -> 13.6 us
    pallas_call x0 -> x3, Pallas kernels: none -> 110 us  [the longest x1 51.4 us: on_device(): pl.pallas_call(mixer_kernel, grid=(heads // per_step,), out_shape=[jax.Sh...]
    all_gather x2 -> x0, blocking collectives: 48.2 us -> none  [the longest x1 25 us: on_device(): section = lax.all_gather(sequence_input_rows, 'ep', axis=0, tiled=True)]
    dot_general x13 -> x0, matrix products: 30.5 us -> none  [the longest x1 13.6 us: token_mixer_step(): jnp.einsum('bhvk,bhk->bhv', value_key_state, removal_dir, precision=lax.P...]
    all_to_all x4 -> x0, waiting for transfers between devices: 21.7 us -> none  [the longest x1 7.72 us: by_exchange(): lax.all_to_all(finished, 'ep', split_axis=0, concat_axis=0, tiled=True)]
    all_to_all x4 -> x0, starting transfers between devices: 14 us -> none  [the longest x1 3.51 us: on_device(): lax.all_to_all(projected, 'ep', split_axis=0, concat_axis=2, tiled=True)]
    unnamed x22 -> x49, local copies, waits for them, and re-layouts: 4.3 us -> 13.6 us
    add x1 -> x0, other arithmetic: 7.89 us -> none  [token_mixer_step(): value_key_state * decay_heads[:, :, None, :]]
    mul x4 -> x0, local copies, waits for them, and re-layouts: 2.39 us -> none  [the longest x1 0.77 us: token_mixer_step(): key_heads * removal_key_scale.reshape(attention_subspace_number, subspace...]
  transfers between devices with their start and end apart: 4 -> 0, of which waited for: 3 -> 0; matrix products, arithmetic and copies ran while one was open for 6% -> 0% of each run, Pallas kernels for 0% -> 0%
where the time goes in v1:
time: 125 us
  Pallas kernels  110 us (88%)
  local copies, waits for them, and re-layouts  13.6 us (11%)
    pallas_call x1, Pallas kernels, on_device(): pl.pallas_call(mixer_kernel, grid=(heads // per_step,), out_shape=[jax.Sh...  51.4 us
    pallas_call x1, Pallas kernels, on_device(): pl.pallas_call(functools.partial(finish_kernel, n), out_shape=jax.ShapeDt...  32.6 us
    pallas_call x1, Pallas kernels, on_device(): pl.pallas_call(functools.partial(project_kernel, n), out_shape=[jax.Shape...  26.4 us
    unnamed x49, local copies, waits for them, and re-layouts  13.6 us

profile of v1, /device:TPU:0, one launch (start us, length us, event | category | flops | bytes accessed | tf_op | source)
XLA Modules:
  0.0 124.8 jit_solution(4350400698325950752)
XLA Ops:
  0.6 0.0 copy-start
  0.6 0.0 copy-start.1
  0.7 0.0 copy-start.2
  0.7 0.0 copy-start.4
  0.7 1.2 copy-done.4
  1.9 0.0 copy-start.5
  1.9 1.0 copy-done.5
  2.9 0.0 copy-start.6
  2.9 1.0 copy-done.6
  3.9 0.0 copy-start.7
  3.9 0.9 copy-done.7
  4.9 0.0 copy-start.8
  4.9 0.9 copy-done.8
  5.8 0.0 copy-start.9
  5.8 0.9 copy-done.9
  6.8 0.0 copy-start.10
  6.8 0.9 copy-done.10
  7.7 0.0 copy-start.12
  7.7 0.8 copy-done.12
  8.5 0.0 copy-start.19
  8.5 0.7 copy-done.19
  9.2 0.0 copy-start.20
  9.2 0.7 copy-done.20
  9.9 0.0 copy-start.23
  9.9 0.0 copy-start.13
  9.9 0.0 copy-start.14
  9.9 0.0 copy-start.21
  9.9 0.0 copy-start.22
  9.9 26.4 %project.1 = (f32[3,8,2048]{2,1,0:T(8,128)S(1)}, f32[8,2048]{1,0:T(8,128)S(1)}, f32[8,2048]{1,0:T(8,128)S(1)}) custom-call(bf16[7,2048]{1,0:T(8,128)(2,1)S(1)} %copy-done.12, bf16[2048,128]{1,0:T(8,128)(2,1)S(1)} %copy-done.4, bf16[2048,128]{1,0:T(8,128)(2,1)S(1)} %copy-done.5, bf16[2048,128]{1,0:T(8,128)(2,1)S(1)} %copy-done.6, ...), custom_call_target="tpu_custom_call" | custom-call | tf_op jit(solution)/shard_map/project/pallas_call | solution.py:354
  36.3 0.0 copy-start.11
  36.3 0.7 copy-done.11
  37.0 0.6 copy-done.15
  37.6 0.6 copy-done.16
  38.2 51.4 %mixer.1 = (bf16[8,2048]{1,0:T(8,128)(2,1)}, f32[7,32,64,64]{3,2,1,0:T(8,128)}) custom-call(f32[7,32,64,64]{3,2,1,0:T(8,128)} %state.1, f32[3,8,2048]{2,1,0:T(8,128)} %copy-done.11, f32[8,2048]{1,0:T(8,128)} %copy-done.15, f32[8,2048]{1,0:T(8,128)} %copy-done.16, f32[1,2048]{1,0:T(1,128)} %bitcast.20, f32[1,2048]{1,0:T(1,128)} %bitcast.21, ...), custom_call_target="tpu_custom_call" | custom-call | tf_op jit(solution)/shard_map/mixer/pallas_call | solution.py:399
  89.7 0.0 copy-done.23
  89.7 0.0 copy-done
  89.7 0.0 copy-done.1
  89.7 0.0 copy-done.2
  89.7 0.0 copy-done.13
  89.7 0.0 copy-done.14
  89.7 0.0 copy-done.18
  89.8 0.0 copy-done.21
  89.8 0.0 copy-done.22
  89.8 0.0 copy-start.3
  89.8 1.0 copy-done.3
  90.8 0.8 copy-done.17
  91.6 32.6 %finish.1 = bf16[7,2048]{1,0:T(8,128)(2,1)S(1)} custom-call(bf16[8,2048]{1,0:T(8,128)(2,1)S(1)} %copy-done.17, bf16[7,2048]{1,0:T(8,128)(2,1)S(1)} %copy-done.13, s32[4,8]{1,0:T(4,128)S(1)} %pad.4.routes, f32[1,2048]{1,0:T(1,128)S(1)} %bitcast.18, bf16[4,2048]{1,0:T(4,128)(2,1)S(1)} %bitcast.15, bf16[16,2048]{1,0:T(8,128)(2,1)S(1)} %bitcast.14, ...), custom_call_target="tpu_custom_call" | custom-call | tf_op jit(solution)/shard_map/finish/pallas_call | solution.py:430
  124.2 0.6 copy.27
  (5 shorter events, 0.0 us)
Async XLA Ops:
  0.6 89.1 %copy-start = (bf16[1,2048,256]{2,1,0:T(8,128)(2,1)S(1)}, bf16[1,2048,256]{2,1,0:T(8,128)(2,1)}, u32[]{:S(2)}) copy-start(bf16[1,2048,256]{2,1,0:T(8,128)(2,1)} %w_gate.1) | copy-start | bytes 3145732
  0.6 89.1 %copy-start.1 = (bf16[1,2048,256]{2,1,0:T(8,128)(2,1)S(1)}, bf16[1,2048,256]{2,1,0:T(8,128)(2,1)}, u32[]{:S(2)}) copy-start(bf16[1,2048,256]{2,1,0:T(8,128)(2,1)} %w_up.1) | copy-start | bytes 3145732
  0.7 89.1 %copy-start.2 = (bf16[1,256,2048]{2,1,0:T(8,128)(2,1)S(1)}, bf16[1,256,2048]{2,1,0:T(8,128)(2,1)}, u32[]{:S(2)}) copy-start(bf16[1,256,2048]{2,1,0:T(8,128)(2,1)} %w_down.1) | copy-start | bytes 3145732
  0.7 1.2 copy-start.4
  1.9 1.0 copy-start.5
  2.9 1.0 copy-start.6
  3.9 0.9 copy-start.7
  4.9 0.9 copy-start.8
  5.8 0.9 copy-start.9
  6.8 0.9 copy-start.10
  7.7 0.8 copy-start.12
  8.5 0.7 copy-start.19
  9.2 0.7 copy-start.20
  9.9 79.8 %copy-start.23 = (s32[7,4]{0,1:T(4,128)S(1)}, s32[7,4]{0,1:T(4,128)}, u32[]{:S(2)}) copy-start(s32[7,4]{0,1:T(4,128)} %param.47) | copy-start | bytes 340
  9.9 79.8 %copy-start.13 = (bf16[7,2048]{1,0:T(8,128)(2,1)S(1)}, bf16[7,2048]{1,0:T(8,128)(2,1)}, u32[]{:S(2)}) copy-start(bf16[7,2048]{1,0:T(8,128)(2,1)} %x_ref.3) | copy-start | bytes 86020
  9.9 79.8 %copy-start.14 = (bf16[2048,16]{0,1:T(8,128)(2,1)S(1)}, bf16[2048,16]{0,1:T(8,128)(2,1)}, u32[]{:S(2)}) copy-start(bf16[2048,16]{0,1:T(8,128)(2,1)} %param.42) | copy-start | bytes 196612
  9.9 79.8 %copy-start.18 = (bf16[2048,4]{0,1:T(4,128)(2,1)S(1)}, bf16[2048,4]{0,1:T(4,128)(2,1)}, u32[]{:S(2)}) copy-start(bf16[2048,4]{0,1:T(4,128)(2,1)} %param.41) | copy-start | bytes 49156
  9.9 79.8 %copy-start.21 = (f32[2048]{0:T(1024)S(1)}, f32[2048]{0:T(1024)}, u32[]{:S(2)}) copy-start(f32[2048]{0:T(1024)} %param.40) | copy-start | bytes 24580
  9.9 79.8 %copy-start.22 = (f32[2048]{0:T(1024)S(1)}, f32[2048]{0:T(1024)}, u32[]{:S(2)}) copy-start(f32[2048]{0:T(1024)} %param.46) | copy-start | bytes 24580
  36.3 0.7 copy-start.11
  37.0 0.6 copy-start.15
  37.6 0.6 copy-start.16
  89.8 1.0 copy-start.3
  90.8 0.8 copy-start.17

commit v2 on v1

--- a/solution.py
+++ b/solution.py
@@ -93,11 +93,65 @@
         each_peer(self.n, self.me, lambda peer: self.incoming(peer).wait_send())
 
 
+class Gather:
+    def __init__(self, n, me, source, landing, send, recv, forward):
+        self.n, self.me, self.source, self.landing = n, me, source, landing
+        self.send, self.recv, self.forward = send, recv, forward
+        self.partner = me + 1 - 2 * lax.rem(me, 2)
+
+    def copy(self, source, slot, sem, peer):
+        return pltpu.make_async_remote_copy(
+            src_ref=source,
+            dst_ref=self.landing.at[slot],
+            send_sem=sem,
+            recv_sem=self.recv.at[slot],
+            device_id={"ep": peer},
+            device_id_type=MESH,
+        )
+
+    def own(self, peer):
+        return self.copy(self.source, self.me, self.send.at[peer], peer)
+
+    def onward(self, slot):
+        return self.copy(self.landing.at[slot], slot, self.forward.at[slot], self.partner)
+
+    def each(self, act):
+        def body(d, carry):
+            act(2 * d)
+            return carry
+
+        lax.fori_loop(1, self.n // 2, body, 0)
+
+    def start(self):
+        self.each(lambda d: self.own(lax.rem(self.me + d, self.n)).start())
+        self.own(self.partner).start()
+
+    def arrive(self, slot, then):
+        self.copy(self.source, slot, self.send.at[slot], slot).wait_recv()
+        then(slot)
+
+    def finish(self, then):
+        def pass_on(d):
+            slot = lax.rem(self.me + self.n - d, self.n)
+            self.copy(self.source, slot, self.send.at[slot], slot).wait_recv()
+            self.onward(slot).start()
+            then(slot)
+
+        self.each(pass_on)
+        self.arrive(self.partner, then)
+        self.each(lambda d: self.arrive(lax.rem(self.partner + self.n - d, self.n), then))
+
+    def wait_send(self):
+        self.own(self.partner).wait_send()
+        self.each(lambda d: self.own(lax.rem(self.me + d, self.n)).wait_send())
+        self.each(lambda d: self.onward(lax.rem(self.me + self.n - d, self.n)).wait_send())
+
+
 def project_kernel(
-    n, x_ref, wr, wk, wv, dli, dlo, dbase, cri, cro, cbase,
+    n, x_hbm, wr, wk, wv, dli, dlo, dbase_hbm, cri, cro, cbase_hbm,
     rkv_out, decay_out, rate_out,
-    weights, dli_v, dlo_v, cri_v, cro_v, gathered, rows, outs, back,
-    local, send1, recv1, send2, recv2,
+    weights, dli_v, dlo_v, cri_v, cro_v, x_ref, dbase, cbase, gathered, rows, outs, back,
+    local, send1, recv1, send2, recv2, forward,
 ):
     me = lax.axis_index("ep")
     series, _ = x_ref.shape
@@ -105,15 +159,17 @@
     loads = [
         pltpu.make_async_copy(src, dst, local.at[i])
         for i, (src, dst) in enumerate([
-            (dli, dli_v), (cri, cri_v), (dlo, dlo_v), (cro, cro_v),
+            (x_hbm, x_ref), (dli, dli_v), (cri, cri_v), (dlo, dlo_v), (cro, cro_v),
+            (dbase_hbm, dbase), (cbase_hbm, cbase),
             (wr, weights.at[0]), (wk, weights.at[1]), (wv, weights.at[2]),
         ])
     ]
     for load in loads:
         load.start()
     enter(n, me)
-    gather = Exchange(n, me, lambda peer: x_ref, gathered, send1, recv1)
-    gather.start_all()
+    loads[0].wait()
+    gather = Gather(n, me, x_ref, gathered, send1, recv1, forward)
+    gather.start()
 
     rows[...] = jnp.zeros_like(rows)
 
@@ -122,17 +178,17 @@
 
     place(me, x_ref[...])
     own = rows[pl.ds(pl.multiple_of(me * PAD, PAD), PAD), :].astype(BF16)
-    for load in loads[:4]:
+    for load in loads[1:7]:
         load.wait()
     decay_low = jnp.tanh(contract(own, dli_v[...], (1, 1))).astype(BF16)
     decay_pre = dbase[...] + contract(decay_low, dlo_v[...], (1, 0))
     decay_out[...] = jnp.exp(sigmoid(decay_pre) * -(2.718281828459045**-0.5))
     iclr_low = contract(own, cri_v[...], (1, 1)).astype(BF16)
     rate_out[...] = sigmoid(cbase[...] + contract(iclr_low, cro_v[...], (1, 0)))
-    for load in loads[4:]:
+    for load in loads[7:]:
         load.wait()
 
-    gather.wait_recv(lambda peer: place(peer, gathered[peer]))
+    gather.finish(lambda peer: place(peer, gathered[peer]))
     lhs = rows[...].astype(BF16)
     for c in range(3):
         columns = jnp.dot(lhs, weights[c], preferred_element_type=F32)
@@ -150,42 +206,89 @@
 
 def mixer_kernel(
     state, rkv, decay_ref, rate_ref, scale_ref, blend_ref, coef_ref, gain_ref,
-    mixed_out, next_out,
+    mixed_out, next_hbm, fresh, store_sem,
 ):
-    step = pl.program_id(0)
-    series, per_step, head, _ = state.shape
-    value_columns = jnp.transpose(rkv[2])
-    lane = lax.broadcasted_iota(jnp.int32, (head, LANES), 1)
-    pieces = []
-    for h in range(per_step):
-        part = slice(h * head, (h + 1) * head)
-        r, k, v = (rkv[c][:, part] for c in range(3))
-        decay, rate = decay_ref[:, part], rate_ref[:, part]
-        scaled = k * scale_ref[:, part]
-        removal = scaled * lax.rsqrt(jnp.sum(scaled * scaled, -1, keepdims=True) + 1e-06)
-        key_mod = k * (1.0 + (rate - 1.0) * blend_ref[:, part])
-        written = removal * rate
-        readouts = jnp.zeros((head, LANES), F32)
-        for t in range(series):
-            row = slice(t, t + 1)
-            block = state[t, h]
-            removed = jnp.sum(block * removal[row], -1, keepdims=True)
-            after = (
-                block * decay[row]
-                - removed * written[row]
-                + value_columns[part, row] * key_mod[row]
+    series, heads, head, _ = state.shape
+    per_step = LANES // head
+    steps = heads // per_step
+
+    def pair(s):
+        return pl.ds(s * per_step, per_step)
+
+    def store(s):
+        return pltpu.make_async_copy(
+            fresh.at[:, pair(s)], next_hbm.at[:, pair(s)], store_sem.at[s]
+        )
+
+    token = lax.broadcasted_iota(jnp.int32, (PAD, head), 0)
+
+    def step(s, carry):
+        block = pl.ds(pl.multiple_of(s * LANES, LANES), LANES)
+        receptance, key, value = (rkv[c, :, block] for c in range(3))
+        decays, rates = decay_ref[:, block], rate_ref[:, block]
+        scales, blends, gains = scale_ref[:, block], blend_ref[:, block], gain_ref[:, block]
+        pieces = []
+        for h in range(per_step):
+            part = slice(h * head, (h + 1) * head)
+            r, k, v = receptance[:, part], key[:, part], value[:, part]
+            decay, rate = decays[:, part], rates[:, part]
+            scaled = k * scales[:, part]
+            removal = scaled * lax.rsqrt(jnp.sum(scaled * scaled, -1, keepdims=True) + 1e-06)
+            key_mod = k * (1.0 + (rate - 1.0) * blends[:, part])
+            written = removal * rate
+            here = s * per_step + h
+            query = decay * r
+            def split(values):
+                big = values.astype(BF16)
+                return big.astype(F32), values - big.astype(F32)
+
+            q_big, q_small = split(query)
+            d_big, d_small = split(removal)
+            probe = jnp.concatenate([q_big, d_big, q_small, d_small], axis=0).astype(BF16)
+            direct = jnp.zeros((PAD, head), F32)
+            removed = jnp.zeros((PAD, head), F32)
+            for t in range(series):
+                old = state[t, here]
+                big = old.astype(BF16)
+                small = (old - big.astype(F32)).astype(BF16)
+                first = contract(probe, big, (1, 1))
+                second = contract(probe[: 2 * PAD], small, (1, 1))
+                sums = first[: 2 * PAD] + first[2 * PAD :] + second
+                direct = jnp.where(token == t, sums[:PAD], direct)
+                removed = jnp.where(token == t, sums[PAD:], removed)
+            m_big, m_small = split(removed)
+            w_big, w_small = split(-written)
+            k_big, k_small = split(key_mod)
+            left = jnp.concatenate([m_big, m_big, m_small, v, v, jnp.zeros_like(v)], axis=0).astype(BF16)
+            for t in range(series):
+                only = token == t
+                right = jnp.concatenate(
+                    [jnp.where(only, x, 0.0) for x in (w_big, w_small, w_big, k_big, k_small)]
+                    + [jnp.zeros_like(v)], axis=0
+                ).astype(BF16)
+                fresh[t, here] = state[t, here] * decay[t : t + 1] + contract(left, right, (0, 0))
+            readout = (
+                direct
+                - removed * jnp.sum(written * r, -1, keepdims=True)
+                + v * jnp.sum(key_mod * r, -1, keepdims=True)
             )
-            next_out[t, h] = after
-            readout = jnp.sum(after * r[row], -1, keepdims=True)
-            readouts = jnp.where(lane == t, readout, readouts)
-        readout = jnp.transpose(readouts)[:PAD]
-        center = jnp.mean(readout, -1, keepdims=True)
-        spread = jnp.mean(jnp.square(readout - center), -1, keepdims=True)
-        standard = (readout - center) * lax.rsqrt(spread + group_eps) * gain_ref[:, part]
-        coef = coef_ref[pl.ds(step * per_step + h, 1), :]
-        present = jnp.sum(r * key_mod * coef, -1, keepdims=True) * v
-        pieces.append(standard + present)
-    mixed_out[...] = jnp.concatenate(pieces, axis=1).astype(BF16)
+            center = jnp.mean(readout, -1, keepdims=True)
+            spread = jnp.mean(jnp.square(readout - center), -1, keepdims=True)
+            standard = (readout - center) * lax.rsqrt(spread + group_eps) * gains[:, part]
+            coef = coef_ref[pl.ds(here, 1), :]
+            present = jnp.sum(r * key_mod * coef, -1, keepdims=True) * v
+            pieces.append(standard + present)
+        mixed_out[:, block] = jnp.concatenate(pieces, axis=1).astype(BF16)
+        store(s).start()
+        return carry
+
+    lax.fori_loop(0, steps, step, 0)
+
+    def drain(s, carry):
+        store(s).wait()
+        return carry
+
+    lax.fori_loop(0, steps, drain, 0)
 
 
 def finish_kernel(
@@ -194,6 +297,7 @@
     tokens_out,
     wo_v, wg_v, wu_v, wd_v, gathered, outs, back, attn, resid, flat, away, arrived, home,
     landed, local, send1, recv1, send2, recv2, send3, recv3, send4, recv4,
+    forward,
 ):
     me = lax.axis_index("ep")
     series, model = x_ref.shape
@@ -210,8 +314,8 @@
     for load in loads:
         load.start()
     enter(n, me)
-    gather = Exchange(n, me, lambda peer: mixed, gathered, send1, recv1)
-    gather.start_all()
+    gather = Gather(n, me, mixed, gathered, send1, recv1, forward)
+    gather.start()
     gathered[me] = mixed[...]
     resid[...] = jnp.zeros_like(resid)
     resid[:series, :] = x_ref[...].astype(F32)
@@ -237,7 +341,7 @@
     repeat = jnp.where((ahead >= 0) & (ahead < CAP), 1.0, 0.0)
 
     loads[0].wait()
-    gather.wait_recv()
+    gather.finish(lambda peer: None)
     lhs = gathered[...].astype(F32).reshape(n * PAD, model).astype(BF16)
     columns = jnp.dot(lhs, wo_v[...], preferred_element_type=F32)
     outs[...] = columns.reshape(n, PAD, width).astype(BF16)
@@ -307,6 +411,7 @@
 
 VMEM = pl.BlockSpec(memory_space=pltpu.VMEM)
 ANY = pl.BlockSpec(memory_space=pl.ANY)
+HBM = pl.BlockSpec(memory_space=pltpu.HBM)
 MIB = 1024 * 1024
 
 
@@ -358,7 +463,7 @@
             jax.ShapeDtypeStruct((PAD, inner), F32),
             jax.ShapeDtypeStruct((PAD, inner), F32),
         ],
-        in_specs=[VMEM, ANY, ANY, ANY, ANY, ANY, VMEM, ANY, ANY, VMEM],
+        in_specs=[HBM] * 10,
         out_specs=[VMEM] * 3,
         scratch_shapes=[
             pltpu.VMEM((3, model, width), BF16),
@@ -366,54 +471,50 @@
             pltpu.VMEM((low_d, inner), BF16),
             pltpu.VMEM((low_a, model), BF16),
             pltpu.VMEM((low_a, inner), BF16),
+            pltpu.VMEM((series, model), BF16),
+            pltpu.VMEM((1, inner), F32),
+            pltpu.VMEM((1, inner), F32),
             pltpu.VMEM((n, series, model), BF16),
             pltpu.VMEM((n * PAD, model), F32),
             pltpu.VMEM((n, 3, PAD, width), BF16),
             pltpu.VMEM((n, 3, PAD, width), BF16),
-            dma((7,)),
+            dma((10,)),
         ]
-        + [dma((n,))] * 4,
+        + [dma((n,))] * 5,
         compiler_params=pltpu.CompilerParams(
-            collective_id=0, has_side_effects=True, vmem_limit_bytes=32 * MIB
+            collective_id=0, has_side_effects=True, vmem_limit_bytes=24 * MIB
         ),
+        cost_estimate=pl.CostEstimate(flops=20_000_000_000, bytes_accessed=40_000_000, transcendentals=0),
         name="project",
     )(
-        sequence_input_rows,
-        receptance_matrix,
-        key_matrix,
-        value_matrix,
-        decay_lowrank_input.T,
-        decay_lowrank_output,
-        row(decay_base_preact),
-        context_rate_input.T,
-        context_rate_output,
-        row(context_rate_base),
-    )
-
-    per_step = LANES // head
-
-    def lanes(rows):
-        return pl.BlockSpec((rows, LANES), lambda s: (0, s))
-
-    state_spec = pl.BlockSpec((series, per_step, head, head), lambda s: (0, s, 0, 0))
+        *(
+            pltpu.with_memory_space_constraint(operand, pltpu.HBM)
+            for operand in (
+                sequence_input_rows,
+                receptance_matrix,
+                key_matrix,
+                value_matrix,
+                decay_lowrank_input.T,
+                decay_lowrank_output,
+                row(decay_base_preact),
+                context_rate_input.T,
+                context_rate_output,
+                row(context_rate_base),
+            )
+        )
+    )
+
+    steps = heads // (LANES // head)
     mixed, next_recurrent_state = pl.pallas_call(
         mixer_kernel,
-        grid=(heads // per_step,),
         out_shape=[
             jax.ShapeDtypeStruct((PAD, inner), BF16),
             jax.ShapeDtypeStruct(value_key_state.shape, F32),
         ],
-        in_specs=[
-            state_spec,
-            pl.BlockSpec((3, PAD, LANES), lambda s: (0, 0, s)),
-            lanes(PAD),
-            lanes(PAD),
-            lanes(1),
-            lanes(1),
-            pl.BlockSpec((heads, head), lambda s: (0, 0)),
-            lanes(1),
-        ],
-        out_specs=[lanes(PAD), state_spec],
+        in_specs=[VMEM] * 8,
+        out_specs=[VMEM, HBM],
+        scratch_shapes=[pltpu.VMEM(value_key_state.shape, F32), dma((steps,))],
+        compiler_params=pltpu.CompilerParams(vmem_limit_bytes=24 * MIB),
         name="mixer",
     )(
         value_key_state,
@@ -446,10 +547,11 @@
         ]
         + [pltpu.VMEM((n, CAP, model), BF16)] * 4
         + [dma((4,))]
-        + [dma((n,))] * 8,
+        + [dma((n,))] * 9,
         compiler_params=pltpu.CompilerParams(
-            collective_id=1, has_side_effects=True, vmem_limit_bytes=32 * MIB
+            collective_id=1, has_side_effects=True, vmem_limit_bytes=24 * MIB
         ),
+        cost_estimate=pl.CostEstimate(flops=20_000_000_000, bytes_accessed=40_000_000, transcendentals=0),
         name="finish",
     )(
         mixed,

time: 125 us -> 67.2 us (0.54)
  Pallas kernels: 110 us -> 65.5 us
  local copies, waits for them, and re-layouts: 13.6 us -> 0.71 us
    pallas_call x1, Pallas kernels: 51.4 us -> 16 us  [on_device(): pl.pallas_call(mixer_kernel, out_shape=[jax.ShapeDtypeStruct((PAD, inner)...]
    unnamed x49 -> x31, local copies, waits for them, and re-layouts: 13.6 us -> 0.7 us
    pallas_call x1, Pallas kernels: 26.4 us -> 20.6 us  [on_device(): pl.pallas_call(functools.partial(project_kernel, n), out_shape=[jax.Shape...]
    pallas_call x1, Pallas kernels: 32.6 us -> 28.9 us  [on_device(): pl.pallas_call(functools.partial(finish_kernel, n), out_shape=jax.ShapeDt...]
where the time goes in v2:
time: 67.2 us; the launch traced here: 67.1 us
  Pallas kernels  65.5 us (97%)
  between operations  0.9 us (1%)
  local copies, waits for them, and re-layouts  0.71 us (1%)
    pallas_call x1, Pallas kernels, on_device(): pl.pallas_call(functools.partial(finish_kernel, n), out_shape=jax.ShapeDt...  28.9 us
    pallas_call x1, Pallas kernels, on_device(): pl.pallas_call(functools.partial(project_kernel, n), out_shape=[jax.Shape...  20.6 us
    pallas_call x1, Pallas kernels, on_device(): pl.pallas_call(mixer_kernel, out_shape=[jax.ShapeDtypeStruct((PAD, inner)...  16 us

profile of v2, /device:TPU:0, one launch (start us, length us, event | category | flops | bytes accessed | tf_op | source)
XLA Modules:
  0.0 67.1 jit_solution(12814952184179917276)
XLA Ops:
  0.6 0.0 copy-start
  0.6 0.0 copy-start.1
  0.7 0.0 copy-start.2
  0.7 0.0 copy-start.3
  0.7 0.0 copy-start.4
  0.7 20.6 %project.1 = (f32[3,8,2048]{2,1,0:T(8,128)S(1)}, f32[8,2048]{1,0:T(8,128)S(1)}, f32[8,2048]{1,0:T(8,128)S(1)}) custom-call(bf16[7,2048]{1,0:T(8,128)(2,1)} %x_ref.1, bf16[2048,128]{1,0:T(8,128)(2,1)} %wr.1, bf16[2048,128]{1,0:T(8,128)(2,1)} %wk.1, bf16[2048,128]{1,0:T(8,128)(2,1)} %wv.1, bf16[64,2048]{1,0:T(8,128)(2,1)} %bitcast.20, bf16[64,2048]{1,0:T(8,128)(2,1)} %dlo.1, ...), custom_call_target="tpu_custom_call" | custom-call | flops 20000000000 | bytes 40000000 | tf_op jit(solution)/shard_map/project/pallas_call | solution.py:459
  21.3 0.0 copy-start.14
  21.3 0.0 copy-start.5
  21.3 0.0 copy-start.6
  21.3 0.0 copy-start.7
  21.3 0.0 copy-start.8
  21.3 0.0 copy-start.9
  21.4 0.0 copy-start.10
  21.4 0.0 copy-start.11
  21.4 0.0 copy-start.12
  21.4 0.0 copy-start.13
  21.4 0.0 copy-done
  21.4 0.0 copy-done.1
  21.4 0.0 copy-done.2
  21.4 0.0 copy-done.3
  21.4 0.0 copy-done.4
  21.5 16.0 %mixer.1 = (bf16[8,2048]{1,0:T(8,128)(2,1)S(1)}, f32[7,32,64,64]{3,2,1,0:T(8,128)}) custom-call(f32[7,32,64,64]{3,2,1,0:T(8,128)S(1)} %copy-done, f32[3,8,2048]{2,1,0:T(8,128)S(1)} %get-tuple-element.7.rkv, f32[8,2048]{1,0:T(8,128)S(1)} %get-tuple-element.8.decay_ref, f32[8,2048]{1,0:T(8,128)S(1)} %get-tuple-element.9.rate_ref, f32[1,2048]{1,0:T(1,128)S(1)} %bitcast.12, ...), custom_call_target="tpu_custom_call" | custom-call | tf_op jit(solution)/shard_map/mixer/pallas_call | solution.py:508
  37.4 0.0 copy-done.14
  37.4 0.0 copy-done.5
  37.4 0.0 copy-done.6
  37.5 0.0 copy-done.7
  37.5 0.0 copy-done.8
  37.5 0.0 copy-done.9
  37.5 0.0 copy-done.10
  37.5 0.0 copy-done.11
  37.5 0.0 copy-done.12
  37.5 0.0 copy-done.13
  37.5 28.9 %finish.1 = bf16[7,2048]{1,0:T(8,128)(2,1)S(1)} custom-call(bf16[8,2048]{1,0:T(8,128)(2,1)S(1)} %get-tuple-element.10.mixed, bf16[7,2048]{1,0:T(8,128)(2,1)S(1)} %copy-done.10, s32[4,8]{1,0:T(4,128)S(1)} %pad.4.routes, f32[1,2048]{1,0:T(1,128)S(1)} %bitcast.17, bf16[4,2048]{1,0:T(4,128)(2,1)S(1)} %bitcast.16, bf16[16,2048]{1,0:T(8,128)(2,1)S(1)} %bitcast.15, ...), custom_call_target="tpu_custom_call" | custom-call | flops 20000000000 | bytes 40000000 | tf_op jit(solution)/shard_map/finish/pallas_call | solution.py:531
  66.5 0.6 copy.27
  (1 shorter events, 0.0 us)
Async XLA Ops:
  0.6 20.8 %copy-start = (f32[7,32,64,64]{3,2,1,0:T(8,128)S(1)}, f32[7,32,64,64]{3,2,1,0:T(8,128)}, u32[]{:S(2)}) copy-start(f32[7,32,64,64]{3,2,1,0:T(8,128)} %state.1) | copy-start | bytes 11010052
  0.6 20.8 %copy-start.1 = (f32[32,64]{1,0:T(8,128)S(1)}, f32[32,64]{1,0:T(8,128)}, u32[]{:S(2)}) copy-start(f32[32,64]{1,0:T(8,128)} %coef_ref.1) | copy-start | bytes 24580
  0.7 20.8 %copy-start.2 = (f32[2048]{0:T(1024)S(1)}, f32[2048]{0:T(1024)}, u32[]{:S(2)}) copy-start(f32[2048]{0:T(1024)} %param.35) | copy-start | bytes 24580
  0.7 20.8 %copy-start.3 = (f32[2048]{0:T(1024)S(1)}, f32[2048]{0:T(1024)}, u32[]{:S(2)}) copy-start(f32[2048]{0:T(1024)} %param.36) | copy-start | bytes 24580
  0.7 20.8 %copy-start.4 = (f32[2048]{0:T(1024)S(1)}, f32[2048]{0:T(1024)}, u32[]{:S(2)}) copy-start(f32[2048]{0:T(1024)} %param.38) | copy-start | bytes 24580
  21.3 16.1 %copy-start.14 = (s32[7,4]{0,1:T(4,128)S(1)}, s32[7,4]{0,1:T(4,128)}, u32[]{:S(2)}) copy-start(s32[7,4]{0,1:T(4,128)} %param.47) | copy-start | bytes 340
  21.3 16.1 %copy-start.5 = (bf16[1,2048,256]{2,1,0:T(8,128)(2,1)S(1)}, bf16[1,2048,256]{2,1,0:T(8,128)(2,1)}, u32[]{:S(2)}) copy-start(bf16[1,2048,256]{2,1,0:T(8,128)(2,1)} %w_gate.1) | copy-start | bytes 3145732
  21.3 16.1 %copy-start.6 = (bf16[1,2048,256]{2,1,0:T(8,128)(2,1)S(1)}, bf16[1,2048,256]{2,1,0:T(8,128)(2,1)}, u32[]{:S(2)}) copy-start(bf16[1,2048,256]{2,1,0:T(8,128)(2,1)} %w_up.1) | copy-start | bytes 3145732
  21.3 16.1 %copy-start.7 = (bf16[1,256,2048]{2,1,0:T(8,128)(2,1)S(1)}, bf16[1,256,2048]{2,1,0:T(8,128)(2,1)}, u32[]{:S(2)}) copy-start(bf16[1,256,2048]{2,1,0:T(8,128)(2,1)} %w_down.1) | copy-start | bytes 3145732
  21.3 16.1 %copy-start.8 = (bf16[2048,128]{1,0:T(8,128)(2,1)S(1)}, bf16[2048,128]{1,0:T(8,128)(2,1)}, u32[]{:S(2)}) copy-start(bf16[2048,128]{1,0:T(8,128)(2,1)} %w_out.1) | copy-start | bytes 1572868
  21.3 16.1 %copy-start.9 = (bf16[2048,16]{0,1:T(8,128)(2,1)S(1)}, bf16[2048,16]{0,1:T(8,128)(2,1)}, u32[]{:S(2)}) copy-start(bf16[2048,16]{0,1:T(8,128)(2,1)} %param.42) | copy-start | bytes 196612
  21.4 16.1 %copy-start.10 = (bf16[7,2048]{1,0:T(8,128)(2,1)S(1)}, bf16[7,2048]{1,0:T(8,128)(2,1)}, u32[]{:S(2)}) copy-start(bf16[7,2048]{1,0:T(8,128)(2,1)} %x_ref.1) | copy-start | bytes 86020
  21.4 16.1 %copy-start.11 = (bf16[2048,4]{0,1:T(4,128)(2,1)S(1)}, bf16[2048,4]{0,1:T(4,128)(2,1)}, u32[]{:S(2)}) copy-start(bf16[2048,4]{0,1:T(4,128)(2,1)} %param.41) | copy-start | bytes 49156
  21.4 16.1 %copy-start.12 = (f32[2048]{0:T(1024)S(1)}, f32[2048]{0:T(1024)}, u32[]{:S(2)}) copy-start(f32[2048]{0:T(1024)} %param.40) | copy-start | bytes 24580
  21.4 16.1 %copy-start.13 = (f32[2048]{0:T(1024)S(1)}, f32[2048]{0:T(1024)}, u32[]{:S(2)}) copy-start(f32[2048]{0:T(1024)} %param.46) | copy-start | bytes 24580

commit v3 on v2

--- a/solution.py
+++ b/solution.py
@@ -209,77 +209,96 @@
     mixed_out, next_hbm, fresh, store_sem,
 ):
     series, heads, head, _ = state.shape
-    per_step = LANES // head
-    steps = heads // per_step
-
-    def pair(s):
-        return pl.ds(s * per_step, per_step)
+    steps, = store_sem.shape
+    per_step = heads // steps
+    span = per_step * head
+    mine = range(per_step)
 
     def store(s):
+        group = pl.ds(s * per_step, per_step)
         return pltpu.make_async_copy(
-            fresh.at[:, pair(s)], next_hbm.at[:, pair(s)], store_sem.at[s]
+            fresh.at[:, group], next_hbm.at[:, group], store_sem.at[s]
         )
 
     token = lax.broadcasted_iota(jnp.int32, (PAD, head), 0)
 
+    def split(values):
+        big = values.astype(BF16)
+        return big.astype(F32), values - big.astype(F32)
+
+    def total(values):
+        return jnp.sum(values, -1, keepdims=True)
+
     def step(s, carry):
-        block = pl.ds(pl.multiple_of(s * LANES, LANES), LANES)
-        receptance, key, value = (rkv[c, :, block] for c in range(3))
-        decays, rates = decay_ref[:, block], rate_ref[:, block]
-        scales, blends, gains = scale_ref[:, block], blend_ref[:, block], gain_ref[:, block]
-        pieces = []
-        for h in range(per_step):
-            part = slice(h * head, (h + 1) * head)
-            r, k, v = receptance[:, part], key[:, part], value[:, part]
-            decay, rate = decays[:, part], rates[:, part]
-            scaled = k * scales[:, part]
-            removal = scaled * lax.rsqrt(jnp.sum(scaled * scaled, -1, keepdims=True) + 1e-06)
-            key_mod = k * (1.0 + (rate - 1.0) * blends[:, part])
-            written = removal * rate
-            here = s * per_step + h
-            query = decay * r
-            def split(values):
-                big = values.astype(BF16)
-                return big.astype(F32), values - big.astype(F32)
-
-            q_big, q_small = split(query)
-            d_big, d_small = split(removal)
-            probe = jnp.concatenate([q_big, d_big, q_small, d_small], axis=0).astype(BF16)
-            direct = jnp.zeros((PAD, head), F32)
-            removed = jnp.zeros((PAD, head), F32)
-            for t in range(series):
-                old = state[t, here]
+        block = pl.ds(pl.multiple_of(s * span, LANES), span)
+
+        def per_head(values):
+            return [values[:, h * head : (h + 1) * head] for h in mine]
+
+        r, k, v = (per_head(rkv[c, :, block]) for c in range(3))
+        decay, rate = per_head(decay_ref[:, block]), per_head(rate_ref[:, block])
+        scale, blend = per_head(scale_ref[:, block]), per_head(blend_ref[:, block])
+        gain = per_head(gain_ref[:, block])
+        scaled = [k[h] * scale[h] for h in mine]
+        norms = [total(scaled[h] * scaled[h]) for h in mine]
+        removal = [scaled[h] * lax.rsqrt(norms[h] + 1e-06) for h in mine]
+        key_mod = [k[h] * (1.0 + (rate[h] - 1.0) * blend[h]) for h in mine]
+        written = [removal[h] * rate[h] for h in mine]
+        coef = [coef_ref[pl.ds(s * per_step + h, 1), :] for h in mine]
+        gone_along = [total(written[h] * r[h]) for h in mine]
+        new_along = [total(key_mod[h] * r[h]) for h in mine]
+        present = [total(r[h] * key_mod[h] * coef[h]) * v[h] for h in mine]
+        probe = []
+        for h in mine:
+            q_big, q_small = split(decay[h] * r[h])
+            d_big, d_small = split(removal[h])
+            probe.append(
+                jnp.concatenate([q_big, d_big, q_small, d_small], axis=0).astype(BF16)
+            )
+        direct = [jnp.zeros((PAD, head), F32) for h in mine]
+        removed = [jnp.zeros((PAD, head), F32) for h in mine]
+        for t in range(series):
+            for h in mine:
+                old = state[t, s * per_step + h]
                 big = old.astype(BF16)
                 small = (old - big.astype(F32)).astype(BF16)
-                first = contract(probe, big, (1, 1))
-                second = contract(probe[: 2 * PAD], small, (1, 1))
+                first = contract(probe[h], big, (1, 1))
+                second = contract(probe[h][: 2 * PAD], small, (1, 1))
                 sums = first[: 2 * PAD] + first[2 * PAD :] + second
-                direct = jnp.where(token == t, sums[:PAD], direct)
-                removed = jnp.where(token == t, sums[PAD:], removed)
-            m_big, m_small = split(removed)
-            w_big, w_small = split(-written)
-            k_big, k_small = split(key_mod)
-            left = jnp.concatenate([m_big, m_big, m_small, v, v, jnp.zeros_like(v)], axis=0).astype(BF16)
-            for t in range(series):
-                only = token == t
+                direct[h] = jnp.where(token == t, sums[:PAD], direct[h])
+                removed[h] = jnp.where(token == t, sums[PAD:], removed[h])
+        left, terms = [], []
+        for h in mine:
+            m_big, m_small = split(removed[h])
+            w_big, w_small = split(-written[h])
+            k_big, k_small = split(key_mod[h])
+            nothing = jnp.zeros_like(v[h])
+            left.append(
+                jnp.concatenate(
+                    [m_big, m_big, m_small, v[h], v[h], nothing], axis=0
+                ).astype(BF16)
+            )
+            terms.append((w_big, w_small, w_big, k_big, k_small, nothing))
+        for t in range(series):
+            for h in mine:
                 right = jnp.concatenate(
-                    [jnp.where(only, x, 0.0) for x in (w_big, w_small, w_big, k_big, k_small)]
-                    + [jnp.zeros_like(v)], axis=0
+                    [jnp.where(token == t, x, 0.0) for x in terms[h]], axis=0
                 ).astype(BF16)
-                fresh[t, here] = state[t, here] * decay[t : t + 1] + contract(left, right, (0, 0))
-            readout = (
-                direct
-                - removed * jnp.sum(written * r, -1, keepdims=True)
-                + v * jnp.sum(key_mod * r, -1, keepdims=True)
-            )
-            center = jnp.mean(readout, -1, keepdims=True)
-            spread = jnp.mean(jnp.square(readout - center), -1, keepdims=True)
-            standard = (readout - center) * lax.rsqrt(spread + group_eps) * gains[:, part]
-            coef = coef_ref[pl.ds(here, 1), :]
-            present = jnp.sum(r * key_mod * coef, -1, keepdims=True) * v
-            pieces.append(standard + present)
+                here = s * per_step + h
+                fresh[t, here] = state[t, here] * decay[h][t : t + 1] + contract(
+                    left[h], right, (0, 0)
+                )
+        store(s).start()
+        readout = [
+            direct[h] - removed[h] * gone_along[h] + v[h] * new_along[h] for h in mine
+        ]
+        center = [total(readout[h]) * (1.0 / head) for h in mine]
+        spread = [total(jnp.square(readout[h] - center[h])) * (1.0 / head) for h in mine]
+        pieces = [
+            (readout[h] - center[h]) * lax.rsqrt(spread[h] + group_eps) * gain[h] + present[h]
+            for h in mine
+        ]
         mixed_out[:, block] = jnp.concatenate(pieces, axis=1).astype(BF16)
-        store(s).start()
         return carry
 
     lax.fori_loop(0, steps, step, 0)
@@ -504,7 +523,7 @@
         )
     )
 
-    steps = heads // (LANES // head)
+    steps = heads // (2 * LANES // head)
     mixed, next_recurrent_state = pl.pallas_call(
         mixer_kernel,
         out_shape=[

time: 67.2 us -> 62 us (0.923)
  Pallas kernels: 65.5 us -> 60.2 us
    pallas_call x1, Pallas kernels: 16 us -> 10.7 us  [on_device(): pl.pallas_call(mixer_kernel, out_shape=[jax.ShapeDtypeStruct((PAD, inner)...]
where the time goes in v3:
time: 62 us; the launch traced here: 61.8 us
  Pallas kernels  60.2 us (97%)
  between operations  0.9 us (1%)
  local copies, waits for them, and re-layouts  0.71 us (1%)
    pallas_call x1, Pallas kernels, on_device(): pl.pallas_call(functools.partial(finish_kernel, n), out_shape=jax.ShapeDt...  28.9 us
    pallas_call x1, Pallas kernels, on_device(): pl.pallas_call(functools.partial(project_kernel, n), out_shape=[jax.Shape...  20.6 us
    pallas_call x1, Pallas kernels, on_device(): pl.pallas_call(mixer_kernel, out_shape=[jax.ShapeDtypeStruct((PAD, inner)...  10.7 us

profile of v3, /device:TPU:0, one launch (start us, length us, event | category | flops | bytes accessed | tf_op | source)
XLA Modules:
  0.0 61.8 jit_solution(3461477477076040125)
XLA Ops:
  0.6 0.0 copy-start
  0.6 0.0 copy-start.1
  0.7 0.0 copy-start.2
  0.7 0.0 copy-start.3
  0.7 0.0 copy-start.4
  0.7 20.6 %project.1 = (f32[3,8,2048]{2,1,0:T(8,128)S(1)}, f32[8,2048]{1,0:T(8,128)S(1)}, f32[8,2048]{1,0:T(8,128)S(1)}) custom-call(bf16[7,2048]{1,0:T(8,128)(2,1)} %x_ref.1, bf16[2048,128]{1,0:T(8,128)(2,1)} %wr.1, bf16[2048,128]{1,0:T(8,128)(2,1)} %wk.1, bf16[2048,128]{1,0:T(8,128)(2,1)} %wv.1, bf16[64,2048]{1,0:T(8,128)(2,1)} %bitcast.20, bf16[64,2048]{1,0:T(8,128)(2,1)} %dlo.1, ...), custom_call_target="tpu_custom_call" | custom-call | flops 20000000000 | bytes 40000000 | tf_op jit(solution)/shard_map/project/pallas_call | solution.py:478
  21.3 0.0 copy-start.14
  21.3 0.0 copy-start.5
  21.3 0.0 copy-start.6
  21.3 0.0 copy-start.7
  21.3 0.0 copy-start.8
  21.3 0.0 copy-start.9
  21.4 0.0 copy-start.10
  21.4 0.0 copy-start.11
  21.4 0.0 copy-start.12
  21.4 0.0 copy-start.13
  21.4 0.0 copy-done
  21.4 0.0 copy-done.1
  21.4 0.0 copy-done.2
  21.4 0.0 copy-done.3
  21.4 0.0 copy-done.4
  21.5 10.7 %mixer.1 = (bf16[8,2048]{1,0:T(8,128)(2,1)S(1)}, f32[7,32,64,64]{3,2,1,0:T(8,128)}) custom-call(f32[7,32,64,64]{3,2,1,0:T(8,128)S(1)} %copy-done, f32[3,8,2048]{2,1,0:T(8,128)S(1)} %get-tuple-element.7.rkv, f32[8,2048]{1,0:T(8,128)S(1)} %get-tuple-element.8.decay_ref, f32[8,2048]{1,0:T(8,128)S(1)} %get-tuple-element.9.rate_ref, f32[1,2048]{1,0:T(1,128)S(1)} %bitcast.12, ...), custom_call_target="tpu_custom_call" | custom-call | tf_op jit(solution)/shard_map/mixer/pallas_call | solution.py:527
  32.2 0.0 copy-done.14
  32.2 0.0 copy-done.5
  32.2 0.0 copy-done.6
  32.2 0.0 copy-done.7
  32.2 0.0 copy-done.8
  32.2 0.0 copy-done.9
  32.3 0.0 copy-done.10
  32.3 0.0 copy-done.11
  32.3 0.0 copy-done.12
  32.3 0.0 copy-done.13
  32.3 28.9 %finish.1 = bf16[7,2048]{1,0:T(8,128)(2,1)S(1)} custom-call(bf16[8,2048]{1,0:T(8,128)(2,1)S(1)} %get-tuple-element.10.mixed, bf16[7,2048]{1,0:T(8,128)(2,1)S(1)} %copy-done.10, s32[4,8]{1,0:T(4,128)S(1)} %pad.4.routes, f32[1,2048]{1,0:T(1,128)S(1)} %bitcast.17, bf16[4,2048]{1,0:T(4,128)(2,1)S(1)} %bitcast.16, bf16[16,2048]{1,0:T(8,128)(2,1)S(1)} %bitcast.15, ...), custom_call_target="tpu_custom_call" | custom-call | flops 20000000000 | bytes 40000000 | tf_op jit(solution)/shard_map/finish/pallas_call | solution.py:550
  61.2 0.6 copy.27
  (1 shorter events, 0.0 us)
Async XLA Ops:
  0.6 20.8 %copy-start = (f32[7,32,64,64]{3,2,1,0:T(8,128)S(1)}, f32[7,32,64,64]{3,2,1,0:T(8,128)}, u32[]{:S(2)}) copy-start(f32[7,32,64,64]{3,2,1,0:T(8,128)} %state.1) | copy-start | bytes 11010052
  0.6 20.8 %copy-start.1 = (f32[32,64]{1,0:T(8,128)S(1)}, f32[32,64]{1,0:T(8,128)}, u32[]{:S(2)}) copy-start(f32[32,64]{1,0:T(8,128)} %coef_ref.1) | copy-start | bytes 24580
  0.7 20.8 %copy-start.2 = (f32[2048]{0:T(1024)S(1)}, f32[2048]{0:T(1024)}, u32[]{:S(2)}) copy-start(f32[2048]{0:T(1024)} %param.35) | copy-start | bytes 24580
  0.7 20.8 %copy-start.3 = (f32[2048]{0:T(1024)S(1)}, f32[2048]{0:T(1024)}, u32[]{:S(2)}) copy-start(f32[2048]{0:T(1024)} %param.36) | copy-start | bytes 24580
  0.7 20.8 %copy-start.4 = (f32[2048]{0:T(1024)S(1)}, f32[2048]{0:T(1024)}, u32[]{:S(2)}) copy-start(f32[2048]{0:T(1024)} %param.38) | copy-start | bytes 24580
  21.3 10.9 %copy-start.14 = (s32[7,4]{0,1:T(4,128)S(1)}, s32[7,4]{0,1:T(4,128)}, u32[]{:S(2)}) copy-start(s32[7,4]{0,1:T(4,128)} %param.47) | copy-start | bytes 340
  21.3 10.9 %copy-start.5 = (bf16[1,2048,256]{2,1,0:T(8,128)(2,1)S(1)}, bf16[1,2048,256]{2,1,0:T(8,128)(2,1)}, u32[]{:S(2)}) copy-start(bf16[1,2048,256]{2,1,0:T(8,128)(2,1)} %w_gate.1) | copy-start | bytes 3145732
  21.3 10.9 %copy-start.6 = (bf16[1,2048,256]{2,1,0:T(8,128)(2,1)S(1)}, bf16[1,2048,256]{2,1,0:T(8,128)(2,1)}, u32[]{:S(2)}) copy-start(bf16[1,2048,256]{2,1,0:T(8,128)(2,1)} %w_up.1) | copy-start | bytes 3145732
  21.3 10.9 %copy-start.7 = (bf16[1,256,2048]{2,1,0:T(8,128)(2,1)S(1)}, bf16[1,256,2048]{2,1,0:T(8,128)(2,1)}, u32[]{:S(2)}) copy-start(bf16[1,256,2048]{2,1,0:T(8,128)(2,1)} %w_down.1) | copy-start | bytes 3145732
  21.3 10.9 %copy-start.8 = (bf16[2048,128]{1,0:T(8,128)(2,1)S(1)}, bf16[2048,128]{1,0:T(8,128)(2,1)}, u32[]{:S(2)}) copy-start(bf16[2048,128]{1,0:T(8,128)(2,1)} %w_out.1) | copy-start | bytes 1572868
  21.3 10.9 %copy-start.9 = (bf16[2048,16]{0,1:T(8,128)(2,1)S(1)}, bf16[2048,16]{0,1:T(8,128)(2,1)}, u32[]{:S(2)}) copy-start(bf16[2048,16]{0,1:T(8,128)(2,1)} %param.42) | copy-start | bytes 196612
  21.4 10.9 %copy-start.10 = (bf16[7,2048]{1,0:T(8,128)(2,1)S(1)}, bf16[7,2048]{1,0:T(8,128)(2,1)}, u32[]{:S(2)}) copy-start(bf16[7,2048]{1,0:T(8,128)(2,1)} %x_ref.1) | copy-start | bytes 86020
  21.4 10.9 %copy-start.11 = (bf16[2048,4]{0,1:T(4,128)(2,1)S(1)}, bf16[2048,4]{0,1:T(4,128)(2,1)}, u32[]{:S(2)}) copy-start(bf16[2048,4]{0,1:T(4,128)(2,1)} %param.41) | copy-start | bytes 49156
  21.4 10.9 %copy-start.12 = (f32[2048]{0:T(1024)S(1)}, f32[2048]{0:T(1024)}, u32[]{:S(2)}) copy-start(f32[2048]{0:T(1024)} %param.40) | copy-start | bytes 24580
  21.4 10.9 %copy-start.13 = (f32[2048]{0:T(1024)S(1)}, f32[2048]{0:T(1024)}, u32[]{:S(2)}) copy-start(f32[2048]{0:T(1024)} %param.46) | copy-start | bytes 24580
